TPU v7x, 256 devices: a whole 4x4x8 slice. The times are simulated.
256 devices in a mesh: ep: 64 (over z, y, core), tp: 4 (over x).
Axes of the slice: x: 4, y: 4, z: 8, core: 2. Of those that a mesh axis runs over, the one named last changes fastest.
Arguments:
- queries: bfloat16 [16384, 1536], P('ep', 'tp'), may hold values from -6 to 6
- kv_latent: bfloat16 [16384, 512], P('ep'), may hold values from -6 to 6
- rope_key: bfloat16 [16384, 64], P('ep'), may hold values from -6 to 6
- latent_gain: float32 [512], replicated, may hold values from 0.1 to 1.9
- w_key_up: bfloat16 [512, 1024], P(None, 'tp'), may hold values from -0.25 to 0.25
- w_value_up: bfloat16 [512, 1024], P(None, 'tp'), may hold values from -0.25 to 0.25
- query_gain: float32 [192], replicated, may hold values from 0.1 to 1.9
- key_gain: float32 [128], replicated, may hold values from 0.1 to 1.9
- rope_gain: float32 [64], replicated, may hold values from 0.1 to 1.9
- out_gain: float32 [128], replicated, may hold values from 0.1 to 1.9
- moe_tokens: bfloat16 [16384, 2048], P('ep'), may hold values from -6 to 6
- moe_gain: float32 [2048], replicated, may hold values from 0.1 to 1.9
- routes: int32 [16384, 2], P('ep'), may hold values from 0 to 63, all different within a row; in each aligned block of 64 rows (0 to 63, 64 to 127, ...) at most 3 rows name the same one
- route_weights: float32 [16384, 2], P('ep'), may hold values from 0.25 to 1
- w_gate: bfloat16 [64, 2048, 3584], P('ep', None, 'tp'), may hold values from -0.125 to 0.125
- w_up: bfloat16 [64, 2048, 3584], P('ep', None, 'tp'), may hold values from -0.125 to 0.125
- w_down: bfloat16 [64, 3584, 2048], P('ep', 'tp'), may hold values from -0.09375 to 0.09375
Outputs:
- attended: bfloat16 [16384, 1024], P('ep', 'tp')
- moe_out: bfloat16 [16384, 2048], P(('ep', 'tp'))
Inputs may be any that keep to these rules, and one draw needn't show every extreme that they name: `routes`: each row names 2 different experts of 0 to 63; in each aligned block of 64 rows no expert is named by more than 3 rows, and in some block one expert is named by exactly 3.
All inputs are finite; a program needn't handle non-finite values.
Results may differ from a plain program's by a relative error of at most 0.0071.
Values may be sent and summed in bfloat16 or wider, within the bound.
A program may use at most 128 MiB of HBM per device.

v0:
```python
import math

import jax
import jax.numpy as jnp
from jax import lax
from jax.sharding import Mesh
from jax.sharding import PartitionSpec as P

EP = ("ep_0", "ep_1", "ep_2")
EP_TP = ("ep_0", "ep_1", "ep_2", "tp")


EPS = 1e-06
THETA = 500000.0


def side_by_side(arrays, axis, dim, along):
    widths = [a.shape[along] for a in arrays]
    both = jnp.concatenate(arrays, axis=along)
    whole = lax.all_gather(both, axis, axis=dim, tiled=True)
    return tuple(jnp.split(whole, [sum(widths[:k]) for k in range(1, len(widths))], axis=along))


def in_blocks(x, dim, count):
    dims = x.shape
    blocks = x.reshape(*dims[:dim], count, dims[dim] // count, *dims[dim + 1 :])
    return jnp.moveaxis(blocks, dim, 0)


def summed_on_arrival(x, axis, dim):
    count = lax.axis_size(axis)
    blocks = lax.all_to_all(in_blocks(x, dim, count), axis, 0, 0, tiled=True)
    return jnp.sum(blocks, axis=0)


def joined_along(blocks, dim):
    blocks = jnp.moveaxis(blocks, 0, dim)
    dims = blocks.shape
    return blocks.reshape(*dims[:dim], dims[dim] * dims[dim + 1], *dims[dim + 2 :])


def moved_by_axis(blocks, axes, order):
    dims = [lax.axis_size(a) for a in axes]
    blocks = blocks.reshape(*dims, *blocks.shape[1:])
    for k in order:
        blocks = lax.all_to_all(blocks, axes[k], split_axis=k, concat_axis=k, tiled=True)
    return blocks.reshape(-1, *blocks.shape[len(axes) :])


def core_and_chips(x, groups, order, split_dim, concat_dim):
    count = lax.axis_size(groups[0]) * lax.axis_size(groups[1])
    blocks = in_blocks(x, split_dim, count)
    return joined_along(moved_by_axis(blocks, groups, order), concat_dim)


def rms_norm(values, norm_gain):
    return values * lax.rsqrt(jnp.mean(values * values, axis=-1, keepdims=True) + EPS) * norm_gain


def rope_tables(positions, rope_dim):
    freqs = 1.0 / THETA ** (jnp.arange(0, rope_dim, 2, dtype=jnp.float32) / rope_dim)
    angles = positions.astype(jnp.float32)[:, None] * freqs[None, :]
    return (jnp.cos(angles), jnp.sin(angles))


def rotate(values, rot_cos, rot_sin):
    half_dim = values.shape[-1] // 2
    first_half = values[..., :half_dim]
    second_half = values[..., half_dim:]
    return jnp.concatenate(
        [
            first_half * rot_cos - second_half * rot_sin,
            second_half * rot_cos + first_half * rot_sin,
        ],
        axis=-1,
    )


def attention_part(
    queries,
    kv_latent,
    rope_key,
    latent_gain,
    w_key_up,
    w_value_up,
    query_gain,
    key_gain,
    rope_gain,
    out_gain,
):
    tok_rows = queries.shape[0]
    nope_dim = key_gain.shape[0]
    value_dim = out_gain.shape[0]
    rope_dim = rope_key.shape[1]
    head_count = w_key_up.shape[1] // nope_dim
    offset = lax.axis_index(EP) * tok_rows
    positions = offset + jnp.arange(tok_rows, dtype=jnp.int32)
    rot_cos, rot_sin = rope_tables(positions, rope_dim)
    latent = rms_norm(kv_latent.astype(jnp.float32), latent_gain).astype(jnp.bfloat16)
    key_nope = jnp.dot(latent, w_key_up, preferred_element_type=jnp.float32).reshape(
        tok_rows, head_count, nope_dim
    )
    key_nope = (
        rms_norm(key_nope, key_gain).astype(jnp.bfloat16).reshape(tok_rows, head_count * nope_dim)
    )
    values = jnp.dot(latent, w_value_up, preferred_element_type=jnp.float32).astype(jnp.bfloat16)
    rot_key = rotate(rms_norm(rope_key.astype(jnp.float32), rope_gain), rot_cos, rot_sin).astype(
        jnp.bfloat16
    )
    keys_values = jnp.concatenate([key_nope, values], axis=1)
    query = rms_norm(
        queries.astype(jnp.float32).reshape(tok_rows, head_count, nope_dim + rope_dim), query_gain
    )
    query_nope = query[..., :nope_dim].astype(jnp.bfloat16)
    query_rope = rotate(query[..., nope_dim:], rot_cos[:, None, :], rot_sin[:, None, :]).astype(
        jnp.bfloat16
    )
    scale = (nope_dim + rope_dim) ** (-0.5)
    last_pos = offset + tok_rows - 1
    initial = (
        jnp.zeros((tok_rows, head_count, value_dim), jnp.float32),
        jnp.zeros((head_count, tok_rows), jnp.float32),
    )
    totals = initial
    key_piece, rope_piece = side_by_side((keys_values, rot_key), EP, 0, 1)
    piece_rows = key_piece.shape[0]
    block_rows = math.gcd(piece_rows, 512)

    def one_block(totals_in, block_index):
        block_first = block_index * block_rows
        kv_block = lax.dynamic_slice_in_dim(key_piece, block_first, block_rows, 0)
        rope_block = lax.dynamic_slice_in_dim(rope_piece, block_first, block_rows, 0)

        def attend(sums_in):
            weighted, denominator = sums_in
            key_block = kv_block[:, : head_count * nope_dim].reshape(
                block_rows, head_count, nope_dim
            )
            value_block = kv_block[:, head_count * nope_dim :].reshape(
                block_rows, head_count, value_dim
            )
            scores = (
                jnp.einsum(
                    "qhd,khd->hqk", query_nope, key_block, preferred_element_type=jnp.float32
                )
                + jnp.einsum(
                    "qhr,kr->hqk", query_rope, rope_block, preferred_element_type=jnp.float32
                )
            ) * scale
            key_pos = block_first + jnp.arange(block_rows, dtype=jnp.int32)
            visible = (positions[:, None] >= key_pos[None, :])[None]
            exp_scores = jnp.where(visible, jnp.exp(scores), 0.0)
            denominator = denominator + jnp.sum(exp_scores, axis=-1)
            weighted = weighted + jnp.einsum(
                "hqk,khd->qhd",
                exp_scores.astype(jnp.bfloat16),
                value_block,
                preferred_element_type=jnp.float32,
            )
            return (weighted, denominator)

        def unchanged(sums_in):
            return sums_in

        return (lax.cond(block_first <= last_pos, attend, unchanged, totals_in), None)

    totals, _ = lax.scan(one_block, totals, jnp.arange(piece_rows // block_rows, dtype=jnp.int32))
    weighted, denominator = totals
    mixed = weighted / jnp.transpose(denominator)[:, :, None]
    return rms_norm(mixed, out_gain).astype(jnp.bfloat16).reshape(tok_rows, head_count * value_dim)


def experts_part(moe_tokens, moe_gain, routes, route_weights, w_gate, w_up, w_down):
    n_rows = moe_tokens.shape[0]
    model_dim = moe_tokens.shape[1]
    top_count = routes.shape[1]
    quarters = lax.axis_size("tp")
    part_rows = n_rows // quarters
    experts = lax.axis_size(EP) * w_gate.shape[0]
    capacity = (3 * top_count * part_rows + 2 * experts - 1) // (2 * experts)
    slot_count = experts * capacity
    normed = rms_norm(moe_tokens.astype(jnp.float32), moe_gain).astype(jnp.bfloat16)
    chosen = routes.reshape(quarters, part_rows * top_count)
    onehot = (chosen[..., None] == jnp.arange(experts, dtype=jnp.int32)).astype(jnp.int32)
    rank = jnp.sum((jnp.cumsum(onehot, axis=1) - onehot) * onehot, axis=-1)
    slots = chosen * capacity + rank
    slot_hit = (slots[..., None] == jnp.arange(slot_count, dtype=jnp.int32)).astype(jnp.bfloat16)
    slot_hit = slot_hit.reshape(quarters, part_rows, top_count, slot_count)
    my_part = lax.axis_index("tp")
    mine_hit = lax.dynamic_index_in_dim(slot_hit, my_part, 0, keepdims=False)
    down_cols = w_down[0]
    own_rows = lax.dynamic_slice_in_dim(normed, my_part * part_rows, part_rows, 0)
    outgoing = jnp.einsum(
        "rs,rd->sd", jnp.sum(mine_hit, axis=1), own_rows, preferred_element_type=jnp.float32
    )
    outgoing = outgoing.astype(jnp.bfloat16).reshape(1, experts, capacity, model_dim)
    arrived = lax.all_gather(
        lax.all_to_all(outgoing, EP, split_axis=1, concat_axis=1, tiled=True),
        "tp",
        axis=0,
        tiled=True,
    )
    gate = jnp.einsum("abcd,df->abcf", arrived, w_gate[0], preferred_element_type=jnp.float32)
    upward = jnp.einsum("abcd,df->abcf", arrived, w_up[0], preferred_element_type=jnp.float32)
    hidden = (jax.nn.silu(gate) * upward).astype(jnp.bfloat16)
    summed = summed_on_arrival(
        jnp.einsum("abcf,fd->abcd", hidden, down_cols, preferred_element_type=jnp.float32), "tp", 0
    ).astype(jnp.bfloat16)
    returned = core_and_chips(summed, (("ep_0", "ep_1"), "ep_2"), (0, 1), 1, 1)
    picked = jnp.einsum(
        "rks,sd->rkd",
        mine_hit,
        returned.reshape(slot_count, model_dim),
        preferred_element_type=jnp.float32,
    )
    own_weights = lax.dynamic_slice_in_dim(route_weights, my_part * part_rows, part_rows, 0)
    return jnp.sum(picked * own_weights[:, :, None], axis=1).astype(jnp.bfloat16)


def on_device(
    queries,
    kv_latent,
    rope_key,
    latent_gain,
    w_key_up,
    w_value_up,
    query_gain,
    key_gain,
    rope_gain,
    out_gain,
    moe_tokens,
    moe_gain,
    routes,
    route_weights,
    w_gate,
    w_up,
    w_down,
):
    attended = attention_part(
        queries,
        kv_latent,
        rope_key,
        latent_gain,
        w_key_up,
        w_value_up,
        query_gain,
        key_gain,
        rope_gain,
        out_gain,
    )
    moe_out = experts_part(moe_tokens, moe_gain, routes, route_weights, w_gate, w_up, w_down)
    return (attended, moe_out)


def solution(mesh):
    finer = Mesh(mesh.devices.reshape(8, 4, 2, mesh.shape["tp"]), ("ep_0", "ep_1", "ep_2", "tp"))
    placed = (
        P(EP, "tp"),
        P(EP, None),
        P(EP, None),
        P(),
        P(None, "tp"),
        P(None, "tp"),
        P(),
        P(),
        P(),
        P(),
        P(EP, None),
        P(),
        P(EP, None),
        P(EP, None),
        P(EP, None, "tp"),
        P(EP, None, "tp"),
        P(EP, "tp", None),
    )
    return jax.shard_map(
        on_device,
        mesh=finer,
        in_specs=placed,
        out_specs=(P(EP, "tp"), P(EP_TP, None)),
        check_vma=False,
    )
```

profile of v0, /device:TPU:249, one launch (start us, length us, event | category | flops | bytes accessed | tf_op | source)
XLA Modules:
  0.0 377.6 jit_solution(7822896285566329880)
XLA Ops:
  8.7 1.5 multiply_reduce_fusion
  10.3 1.5 convert_element_type.87
  14.1 34.2 %all_to_all.20 = bf16[1,64,3,2048]{3,2,0,1:T(4,128)(2,1)S(1)} all-to-all(bf16[1,64,3,2048]{3,2,0,1:T(4,128)(2,1)S(1)} %bitcast.98), channel_id=1, replica_groups=mesh['ep_0'=8,'ep_1'=4,'ep_2'=2,'tp'=4] {'ep_0','ep_1','ep_2'}, dimensions={1} | all-to-all | bytes 1572864 | tf_op jit(solution)/shard_map/all_to_all | solution.py:198
  48.4 1.5 copy.56
  52.1 40.0 %all-gather.5.cloned.1.call-done = bf16[4,64,3,2048]{3,1,2,0:T(8,128)(2,1)} async-done(((bf16[1,64,3,2048]{3,1,2,0:T(8,128)(2,1)}), bf16[4,64,3,2048]{3,1,2,0:T(8,128)(2,1)}) %all-gather.5.cloned.1.call-update) | async-done | bytes 3145744 | tf_op jit(solution)/shard_map/all_gather | solution.py:197
  92.2 8.2 %fusion.12 = f32[4,64,3,896]{3,1,2,0:T(8,128)} fusion(bf16[4,64,3,2048]{3,1,2,0:T(8,128)(2,1)} %all-gather.5.cloned.1.call-done, bf16[1,2048,896]{2,1,0:T(8,128)(2,1)} %param.36), kind=kOutput, calls=%fused_computation.20 | convolution fusion | flops 2818572288 | bytes 9568256 | tf_op jit(solution)/shard_map/abcd,df->abcf/dot_general | solution.py:204
  100.3 13.4 %convolution_bitcast_fusion.3 = f32[4,1,64,3,2048]{4,2,3,1,0:T(8,128)} fusion(bf16[1,896,2048]{2,1,0:T(8,128)(2,1)} %param.37, f32[4,64,3,896]{3,1,2,0:T(8,128)} %fusion.12, bf16[4,64,3,2048]{3,1,2,0:T(8,128)(2,1)S(1)} %copy-done.10, bf16[1,2048,896]{2,1,0:T(8,128)(2,1)} %param.35), kind=kOutput, calls=%fused_computation.18 | convolution fusion | flops 5641273344 | bytes 19529728 | tf_op jit(solution)/shard_map/abcf,fd->abcd/dot_general | solution.py:207
  113.7 74.3 %all_to_all.21 = f32[4,1,64,3,2048]{4,2,3,1,0:T(8,128)S(1)} all-to-all(f32[4,1,64,3,2048]{4,2,3,1,0:T(8,128)} %convolution_bitcast_fusion.3), channel_id=1, replica_groups=mesh['ep_0'=8,'ep_1'=4,'ep_2'=2,'tp'=4] {'tp'}, dimensions={0} | all-to-all | bytes 12582912 | tf_op jit(solution)/shard_map/all_to_all | solution.py:32
  189.1 1.5 copy.59
  190.6 9.0 %all-to-all-start.2 = ((bf16[32,2,1,1,3,2048]{5,1,4,3,2,0:T(2,128)(2,1)}), bf16[32,2,1,1,3,2048]{5,1,4,3,2,0:T(2,128)(2,1)S(1)}, u32[]{:S(2)}, u32[]{:S(2)}) async-start(bf16[32,2,1,1,3,2048]{5,1,4,3,2,0:T(2,128)(2,1)} %copy.59), calls=%async_computation.2 | async-start | bytes 1572864 | tf_op jit(solution)/shard_map/all_to_all | solution.py:46
  200.2 15.0 %all-to-all-done.2 = bf16[32,2,1,1,3,2048]{5,1,4,3,2,0:T(2,128)(2,1)S(1)} async-done(((bf16[32,2,1,1,3,2048]{5,1,4,3,2,0:T(2,128)(2,1)}), bf16[32,2,1,1,3,2048]{5,1,4,3,2,0:T(2,128)(2,1)S(1)}, u32[]{:S(2)}, u32[]{:S(2)}) %all-to-all-start.2) | async-done | bytes 786464 | tf_op jit(solution)/shard_map/all_to_all | solution.py:46
  215.5 8.3 %all_to_all.22 = bf16[32,2,1,1,3,2048]{5,0,4,3,2,1:T(8,128)(2,1)S(1)} all-to-all(bf16[32,2,1,1,3,2048]{5,0,4,3,2,1:T(8,128)(2,1)S(1)} %copy.60), channel_id=1, replica_groups=mesh['ep_0'=8,'ep_1'=4,'ep_2'=2,'tp'=4] {'ep_2'}, dimensions={1} | all-to-all | bytes 1572864 | tf_op jit(solution)/shard_map/all_to_all | solution.py:46
  226.2 1.7 split.9
  228.0 13.8 %split.8 = bf16[16384,512]{0,1:T(8,128)(2,1)} slice(bf16[16384,576]{0,1:T(8,128)(2,1)} %all-gather.3.cloned.1.call-done), slice={[0:16384], [0:512]} | slice | bytes 33554432 | tf_op jit(solution)/shard_map/split | solution.py:21
  241.8 127.8 %while.13 = (s32[]{:T(128)}, f32[256,2,128]{2,0,1:T(8,128)S(1)}, f32[2,256]{1,0:T(2,128)S(1)}, s32[32]{0:T(128)S(1)}, s32[]{:T(128)}, /*index=5*/bf16[16384,512]...) while((s32[]{:T(128)}, f32[256,2,128]{2,0,1:T(8,128)S(1)}, ...), condition=%wide.region_8.9_spmd.clone, body=%wide.region_4.8_spmd.clone.sunk | while | flops 169280256 | bytes 5783893 | solution.py:167
  242.9 2.8 conditional.3
  243.1 1.3 constant_dynamic-slice_fusion
  246.9 2.8 conditional.3
  250.9 2.8 conditional.3
  254.9 2.8 conditional.3
  258.9 2.8 conditional.3
  262.9 2.8 conditional.3
  266.9 2.8 conditional.3
  270.9 2.8 conditional.3
  274.9 2.8 conditional.3
  278.9 2.8 conditional.3
  282.9 2.8 conditional.3
  286.9 2.8 conditional.3
  290.9 2.8 conditional.3
  294.9 2.8 conditional.3
  298.9 2.8 conditional.3
  302.9 2.8 conditional.3
  306.9 2.8 conditional.3
  310.9 2.8 conditional.3
  314.9 2.8 conditional.3
  318.9 2.8 conditional.3
  322.9 2.8 conditional.3
  326.8 2.8 conditional.3
  330.8 2.8 conditional.3
  334.8 2.8 conditional.3
  338.8 2.8 conditional.3
  342.8 2.8 conditional.3
  346.8 2.8 conditional.3
  350.8 2.8 conditional.3
  354.8 2.8 conditional.3
  358.8 2.8 conditional.3
  362.8 2.8 conditional.3
  366.8 2.8 conditional.3
  (404 shorter events, 116.4 us)
Async XLA Ops:
  7.2 42.9 %copy-start = (bf16[512,256]{1,0:T(8,128)(2,1)S(1)}, bf16[512,256]{1,0:T(8,128)(2,1)}, u32[]{:S(2)}) copy-start(bf16[512,256]{1,0:T(8,128)(2,1)} %param.25) | copy-start | bytes 786436
  7.2 5.9 %copy-start.5 = (f32[2048]{0:T(1024)S(1)}, f32[2048]{0:T(1024)}, u32[]{:S(2)}) copy-start(f32[2048]{0:T(1024)} %param.32) | copy-start | bytes 24580
  7.2 85.0 %all-gather.5.cloned.1.call-start = ((), (), s32[]{:S(2)}) async-start(), calls=%async_computation.5 | async-start | bytes 3932160 | tf_op jit(solution)/shard_map/all_gather | solution.py:197
  13.5 36.4 %copy-start.2 = (bf16[256,512]{1,0:T(8,128)(2,1)S(1)}, bf16[256,512]{1,0:T(8,128)(2,1)}, u32[]{:S(2)}) copy-start(bf16[256,512]{1,0:T(8,128)(2,1)} %param.22) | copy-start | bytes 786436
  13.5 36.5 %copy-start.13 = (f32[128]{0:T(128)S(1)}, f32[128]{0:T(128)}, u32[]{:S(2)}) copy-start(f32[128]{0:T(128)} %param.28) | copy-start | bytes 1540
  13.6 36.6 %copy-start.12 = (f32[512]{0:T(512)S(1)}, f32[512]{0:T(512)}, u32[]{:S(2)}) copy-start(f32[512]{0:T(512)} %param.24) | copy-start | bytes 6148
  14.1 36.6 %copy-start.4 = (bf16[256,64]{0,1:T(8,128)(2,1)S(1)}, bf16[256,64]{0,1:T(8,128)(2,1)}, u32[]{:S(2)}) copy-start(bf16[256,64]{0,1:T(8,128)(2,1)} %param.23) | copy-start | bytes 98308
  14.1 36.6 %copy-start.7 = (f32[64]{0:T(128)S(1)}, f32[64]{0:T(128)}, u32[]{:S(2)}) copy-start(f32[64]{0:T(128)} %param.29) | copy-start | bytes 772
  14.1 36.9 %copy-start.11 = (bf16[512,256]{1,0:T(8,128)(2,1)S(1)}, bf16[512,256]{1,0:T(8,128)(2,1)}, u32[]{:S(2)}) copy-start(bf16[512,256]{1,0:T(8,128)(2,1)} %param.26) | copy-start | bytes 786436
  49.9 176.4 %all-gather.3.cloned.1.call-start = ((), (), s32[]{:S(2)}) async-start(), calls=%async_computation.4 | async-start | bytes 19169280 | tf_op jit(solution)/shard_map/all_gather | solution.py:20
  92.2 8.2 %copy-start.10 = (bf16[4,64,3,2048]{3,1,2,0:T(8,128)(2,1)S(1)}, bf16[4,64,3,2048]{3,1,2,0:T(8,128)(2,1)}, u32[]{:S(2)}) copy-start(bf16[4,64,3,2048]{3,1,2,0:T(8,128)(2,1)} %all-gather.5.cloned.1.call-done) | copy-start | bytes 9437188
  188.6 11.0 %copy-start.3 = (bf16[256,384]{1,0:T(8,128)(2,1)S(1)}, bf16[256,384]{1,0:T(8,128)(2,1)}, u32[]{:S(2)}) copy-start(bf16[256,384]{1,0:T(8,128)(2,1)} %param.21) | copy-start | bytes 589828
  188.6 11.2 %copy-start.6 = (f32[192]{0:T(256)S(1)}, f32[192]{0:T(256)}, u32[]{:S(2)}) copy-start(f32[192]{0:T(256)} %param.27) | copy-start | bytes 2308
  188.6 11.5 %copy-start.9 = (f32[256,2]{0,1:T(2,128)S(1)}, f32[256,2]{0,1:T(2,128)}, u32[]{:S(2)}) copy-start(f32[256,2]{0,1:T(2,128)} %param.34) | copy-start | bytes 6148
  190.6 24.7 %all-to-all-start.2 = ((bf16[32,2,1,1,3,2048]{5,1,4,3,2,0:T(2,128)(2,1)}), bf16[32,2,1,1,3,2048]{5,1,4,3,2,0:T(2,128)(2,1)S(1)}, u32[]{:S(2)}, u32[]{:S(2)}) async-start(bf16[32,2,1,1,3,2048]{5,1,4,3,2,0:T(2,128)(2,1)} %copy.59), calls=%async_computation.2 | async-start | bytes 1572864 | tf_op jit(solution)/shard_map/all_to_all | solution.py:46
  241.7 128.1 %copy-start.8 = (f32[128]{0:T(128)S(1)}, f32[128]{0:T(128)}, u32[]{:S(2)}) copy-start(f32[128]{0:T(128)} %param.30) | copy-start | bytes 1540
  369.6 1.2 copy-start.1
Sparse Core Ops, SparseCore 0:
  50.0 42.1 all-gather.4
  94.8 109.2 all-gather.2
where the time goes:
time: 379 us; the launch traced here: 378 us
  blocking collectives  117 us (31%)
  local copies, waits for them, and re-layouts  84.3 us (22%)
  matrix products  63.4 us (17%)
  waiting for transfers between devices  55.1 us (15%)
  loops' own time  21.5 us (6%)
  between operations  14.5 us (4%)
  other arithmetic  12.8 us (3%)
  starting transfers between devices  9.09 us (2%)
    all_to_all x1, blocking collectives, summed_on_arrival(): blocks = lax.all_to_all(in_blocks(x, dim, count), axis, 0, 0, tiled=True)  74.3 us
    slice x32, local copies, waits for them, and re-layouts, attend(): kv_block[:, :head_count * nope_dim]  42.8 us
    all_gather x1, waiting for transfers between devices, experts_part(): lax.all_gather(lax.all_to_all(outgoing, EP, split_axis=1, concat_axis=1,...  40 us
    all_to_all x1, blocking collectives, experts_part(): lax.all_to_all(outgoing, EP, split_axis=1, concat_axis=1, tiled=True)  34.2 us
    another operation x1, loops' own time, attention_part(): lax.scan(one_block, totals, jnp.arange(piece_rows // block_rows, dtype=jn...  19.3 us
    dynamic_slice x32, local copies, waits for them, and re-layouts, attention_part(): lax.scan(one_block, totals, jnp.arange(piece_rows // block_rows, dtype=jn...  18.5 us
    dot_general x32, matrix products, attend(): jnp.einsum('qhr,kr->hqk', query_rope, rope_block, preferred_element_type=...  17.2 us
    split x2, local copies, waits for them, and re-layouts, side_by_side(): jnp.split(whole, [sum(widths[:k]) for k in range(1, len(widths))], axis=a...  15.5 us
  transfers between devices with their start and end apart: 3, of which 2 were waited for; matrix products, arithmetic and copies ran while one was open for 8% of the time, Pallas kernels for 0%

commit v1 on v0

--- a/solution.py
+++ b/solution.py
@@ -1,10 +1,17 @@
+import functools
 import math
 
 import jax
 import jax.numpy as jnp
+import numpy as np
 from jax import lax
+from jax.experimental import pallas as pl
+from jax.experimental.pallas import tpu as pltpu
 from jax.sharding import Mesh
 from jax.sharding import PartitionSpec as P
+
+BF, F32, I32 = jnp.bfloat16, jnp.float32, jnp.int32
+MESH = pl.DeviceIdType.MESH
 
 EP = ("ep_0", "ep_1", "ep_2")
 EP_TP = ("ep_0", "ep_1", "ep_2", "tp")
@@ -170,51 +177,448 @@
     return rms_norm(mixed, out_gain).astype(jnp.bfloat16).reshape(tok_rows, head_count * value_dim)
 
 
+SRC = 8
+MSG = 16
+CAP = 12
+
+
+def split_two(v):
+    hi = v.astype(BF)
+    return hi, (v - hi.astype(F32)).astype(BF)
+
+
+def fixed_selects():
+    packed = np.arange(16 * MSG)
+    slot = np.arange(16 * CAP)
+    src, s = slot // CAP, slot % CAP
+    main = (src * MSG + s)[:, None] == packed[None, :]
+    extra = [((src * MSG + CAP + s % 4)[:, None] == packed[None, :]) & (s // 4 == j)[:, None] for j in range(3)]
+    unpack_extra = np.concatenate(extra, axis=1)
+    pack_extra = np.concatenate([e.T for e in extra], axis=0)
+    return [jnp.asarray(a.astype(np.float32), BF) for a in (main, unpack_extra, main.T, pack_extra)]
+
+
+class Place:
+    def __init__(self, n_z):
+        self.n_z = n_z
+        self.z = lax.axis_index("ep_0")
+        self.y = lax.axis_index("ep_1")
+        self.c = lax.axis_index("ep_2")
+        self.t = lax.axis_index("tp")
+        self.s8 = self.y * 2 + self.c
+
+    def row(self, order):
+        up = order % 2
+        return up * ((order + 1) // 2) + (1 - up) * ((self.n_z - order // 2) % self.n_z)
+
+    def x(self, step):
+        return (self.z, self.y, self.c, (self.t + step) % 4)
+
+    def at(self, z, s8):
+        return (z, s8 // 2, s8 % 2, self.t)
+
+
+def greet(pl_, n_z):
+    barrier = pltpu.get_barrier_semaphore()
+
+    def one(i, _):
+        z, s = (pl_.z + i // SRC) % n_z, (pl_.s8 + i % SRC) % SRC
+        pl.semaphore_signal(barrier, inc=1, device_id=pl_.at(z, s), device_id_type=MESH)
+        return 0
+
+    lax.fori_loop(1, n_z * SRC, one, 0)
+    for step in (1, 2, 3):
+        pl.semaphore_signal(barrier, inc=1, device_id=pl_.x(step), device_id_type=MESH)
+
+
+def met(n_z):
+    pl.semaphore_wait(pltpu.get_barrier_semaphore(), n_z * SRC - 1 + 3)
+
+
+def remote(src, dst, send, recv, device):
+    return pltpu.make_async_remote_copy(
+        src_ref=src, dst_ref=dst, send_sem=send, recv_sem=recv, device_id=device, device_id_type=MESH
+    )
+
+
+def await_bytes(ref, sem):
+    pltpu.make_async_copy(ref, ref, sem).wait()
+
+
+def dot(a, b):
+    return jnp.dot(a, b, preferred_element_type=F32)
+
+
+def experts_kernel(
+    n_z,
+    tokens,
+    gain,
+    routes,
+    routes_t,
+    weights,
+    un_main,
+    un_extra,
+    pk_main,
+    pk_extra,
+    wg_hbm,
+    wu_hbm,
+    wd_hbm,
+    out,
+    wg,
+    wu,
+    wd,
+    normed,
+    outb,
+    arr,
+    rows,
+    gacc,
+    uacc,
+    hid,
+    wmix,
+    far,
+    to_r,
+    to_l,
+    relay,
+    from_l,
+    from_r,
+    retb,
+    reti,
+    fino,
+    fini,
+    w_sem,
+    own_sem,
+    out_sem,
+    self_sem,
+    xs_sem,
+    xr_sem,
+    rs_send,
+    relay_sem,
+    fl_sem,
+    fr_sem,
+    ret_send,
+    ret_sem,
+    fin_send,
+    fin_sem,
+):
+    me = Place(n_z)
+    greet(me, n_z)
+    loads = [
+        pltpu.make_async_copy(h.at[0], v, w_sem.at[k]) for k, (h, v) in enumerate(((wg_hbm, wg), (wu_hbm, wu), (wd_hbm, wd)))
+    ]
+    for load in loads:
+        load.start()
+    n_rows, model = tokens.shape
+    cols = model // 4
+    quarter = n_rows // 4
+
+    exp_ids = lax.broadcasted_iota(I32, (64, n_rows), 0)
+    ra, rb = routes_t[0:1, :], routes_t[1:2, :]
+    hit_a, hit_b = exp_ids == ra, exp_ids == rb
+    both = jnp.where(hit_a | hit_b, 1.0, 0.0).astype(BF)
+    i0 = lax.broadcasted_iota(I32, (n_rows, n_rows), 0)
+    i1 = lax.broadcasted_iota(I32, (n_rows, n_rows), 1)
+    same = (i0 // quarter) == (i1 // quarter)
+    earlier_t = jnp.where((i0 < i1) & same, 1.0, 0.0).astype(BF)
+    count_t = dot(both, earlier_t)
+    base_t = lax.broadcasted_iota(I32, (1, n_rows), 1) // quarter * 3
+
+    def places(hit, chosen):
+        s = base_t + jnp.sum(jnp.where(hit, count_t, 0.0), axis=0, keepdims=True).astype(I32)
+        return chosen * MSG + s, chosen * MSG + CAP + s % 4 + 2048 * (s // 4)
+
+    (ma, xa), (mb, xb) = places(hit_a, ra), places(hit_b, rb)
+
+    v = tokens[...].astype(F32)
+    scale = lax.rsqrt(jnp.mean(v * v, axis=-1, keepdims=True) + EPS)
+    mine = pl.ds(pl.multiple_of(me.t * cols, cols), cols)
+    normed[...] = (tokens[:, mine].astype(F32) * scale * gain[:, mine]).astype(BF)
+
+    met(n_z)
+
+    def dispatch(o, _):
+        z = (me.z + me.row(o)) % n_z
+        first = z * SRC * MSG
+        ids = lax.broadcasted_iota(I32, (SRC * MSG, n_rows), 0) + first
+        main = jnp.where((ids == ma) | (ids == mb), 1.0, 0.0).astype(BF)
+        block = dot(main, normed[:, : 3 * 128])
+        extra = []
+        for j in range(3):
+            idj = ids + 2048 * j
+            sel = jnp.where((idj == xa) | (idj == xb), 1.0, 0.0).astype(BF)
+            extra.append(dot(sel, normed[:, 3 * 128 :]))
+        block = block + jnp.concatenate(extra, axis=1)
+        outb[o] = block.astype(BF).reshape(SRC, MSG, 3 * 128)
+
+        def send(i, _):
+            s = (me.s8 + i) % SRC
+            remote(outb.at[o, s], arr.at[0, o, me.s8], out_sem, own_sem.at[o], me.at(z, s)).start()
+            return 0
+
+        lax.fori_loop(jnp.where(o == 0, 1, 0), SRC, send, 0)
+        return 0
+
+    lax.fori_loop(0, n_z, dispatch, 0)
+    pltpu.make_async_copy(outb.at[0, me.s8], arr.at[0, 0, me.s8], own_sem.at[0]).start()
+
+    lane_e = lax.broadcasted_iota(I32, (n_rows, 128), 1)
+    ca, cb = routes[:, 0:1], routes[:, 1:2]
+    on_a, on_b = lane_e == ca, lane_e == cb
+    earlier = jnp.where((i1 < i0) & same, 1.0, 0.0).astype(BF)
+    count = dot(earlier, jnp.where(on_a | on_b, 1.0, 0.0).astype(BF))
+    base = lax.broadcasted_iota(I32, (n_rows, 1), 0) // quarter * 3
+    wa, wb = weights[:, 0:1], weights[:, 1:2]
+
+    def places_c(hit, chosen):
+        s = base + jnp.sum(jnp.where(hit, count, 0.0), axis=1, keepdims=True).astype(I32)
+        return chosen * MSG + s, chosen * MSG + CAP + s % 4 + 2048 * (s // 4)
+
+    (cma, cxa), (cmb, cxb) = places_c(on_a, ca), places_c(on_b, cb)
+
+    def mix(k, _):
+        lanes = lax.broadcasted_iota(I32, (n_rows, 64 * MSG), 1)
+        idk = lanes + 2048 * (k - 1)
+        pa, pb = jnp.where(k == 0, cma - 2048, cxa), jnp.where(k == 0, cmb - 2048, cxb)
+        w = jnp.where(idk == pa, wa, 0.0) + jnp.where(idk == pb, wb, 0.0)
+        hi, lo = split_two(w)
+        wmix[k, 0] = hi
+        wmix[k, 1] = lo
+        return 0
+
+    lax.fori_loop(0, 4, mix, 0)
+
+    def pass_on(b, o, step, dst):
+        remote(arr.at[b, o], arr.at[dst, o], xs_sem.at[b, step % 4 // 2], xr_sem.at[dst - 1, o], me.x(step)).start()
+
+    def unpack(b, p):
+        packed = arr[b, pl.ds(2 * p, 2)].reshape(2 * SRC * MSG, 3 * 128)
+        tiles = jnp.concatenate([packed[:, 128 * j : 128 * (j + 1)] for j in range(3)], axis=0)
+        r = pl.ds(pl.multiple_of(p * 192, 192), 192)
+        rows[b, r, : 3 * 128] = dot(un_main[...], packed).astype(BF)
+        rows[b, r, 3 * 128 :] = dot(un_extra[...], tiles).astype(BF)
+
+    def gather(o, _):
+        await_bytes(arr.at[0, o], own_sem.at[o])
+        pass_on(0, o, 1, 1)
+        pass_on(0, o, 3, 2)
+
+        @pl.when(o % 2 == 1)
+        def _():
+            unpack(0, o // 2)
+
+        return 0
+
+    def relay_on(o):
+        await_bytes(arr.at[1, o], xr_sem.at[0, o])
+        await_bytes(arr.at[2, o], xr_sem.at[1, o])
+
+        @pl.when(o % 2 == 0)
+        def _():
+            pass_on(1, o, 1, 3)
+
+        @pl.when(o % 2 == 1)
+        def _():
+            pass_on(2, o, 3, 3)
+            unpack(1, o // 2)
+            unpack(2, o // 2)
+
+    def gather_step(o, _):
+        gather(o, 0)
+        relay_on(o - 1)
+        return 0
+
+    gather(0, 0)
+    lax.fori_loop(1, n_z, gather_step, 0)
+    relay_on(n_z - 1)
+
+    loads[0].wait()
+    loads[1].wait()
+    n_all = rows.shape[1]
+    part = 192
+    sides = ((0, 0), (1, 3), (2, 1), (3, 2))
+
+    def up_gate(b, rank, first):
+        k = pl.ds(pl.multiple_of((me.t + rank) % 4 * cols, cols), cols)
+
+        def one(m, _):
+            r = pl.ds(pl.multiple_of(m * part, part), part)
+            lhs = rows[b, r]
+            g, u = dot(lhs, wg[k, :]), dot(lhs, wu[k, :])
+            if first:
+                gacc[r] = g
+                uacc[r] = u
+            else:
+                gacc[r] += g
+                uacc[r] += u
+            return 0
+
+        lax.fori_loop(0, n_all // part, one, 0)
+
+    up_gate(0, 0, True)
+    up_gate(1, 3, False)
+    up_gate(2, 1, False)
+
+    def last_pair(p, _):
+        await_bytes(arr.at[3, 2 * p], xr_sem.at[2, 2 * p])
+        await_bytes(arr.at[3, 2 * p + 1], xr_sem.at[2, 2 * p + 1])
+        unpack(3, p)
+        return 0
+
+    lax.fori_loop(0, n_z // 2, last_pair, 0)
+    k3 = pl.ds(pl.multiple_of((me.t + 2) % 4 * cols, cols), cols)
+
+    def act(m, _):
+        r = pl.ds(pl.multiple_of(m * part, part), part)
+        lhs = rows[3, r]
+        g = gacc[r] + dot(lhs, wg[k3, :])
+        u = uacc[r] + dot(lhs, wu[k3, :])
+        hid[r] = (g / (1.0 + jnp.exp(-g)) * u).astype(BF)
+        return 0
+
+    lax.fori_loop(0, n_all // part, act, 0)
+    loads[2].wait()
+
+    def down(q, rank):
+        return dot(hid[q * part : (q + 1) * part], wd[:, pl.ds(pl.multiple_of((me.t + rank) % 4 * cols, cols), cols)])
+
+    def send_far(q):
+        far[q] = down(q, 2).astype(BF)
+        remote(far.at[q], relay.at[q], rs_send.at[0, q], relay_sem.at[q], me.x(1 if q < 2 else 3)).start()
+
+    def send_side(q, right, add):
+        buf, dst, sem, rank = (to_r, from_l, fl_sem, 1) if right else (to_l, from_r, fr_sem, 3)
+        y = down(q, rank)
+        if add:
+            await_bytes(relay.at[q], relay_sem.at[q])
+            y = y + relay[q].astype(F32)
+        buf[q] = y.astype(BF)
+        remote(buf.at[q], dst.at[q], rs_send.at[1 if right else 2, q], sem.at[q], me.x(1 if right else 3)).start()
+
+    def finish(q):
+        y = down(q, 0)
+        await_bytes(from_l.at[q], fl_sem.at[q])
+        await_bytes(from_r.at[q], fr_sem.at[q])
+        y = (y + from_l[q].astype(F32) + from_r[q].astype(F32)).astype(BF)
+        ext = dot(pk_extra[...], y[:, 3 * 128 :])
+        packed = dot(pk_main[...], y[:, : 3 * 128]) + jnp.concatenate([ext[256 * j : 256 * (j + 1)] for j in range(3)], axis=1)
+        retb[2 * q : 2 * q + 2] = packed.astype(BF).reshape(2, SRC, MSG, 3 * 128)
+        mine_e = me.z * SRC + me.s8
+        for o in (2 * q, 2 * q + 1):
+            z = (me.z - me.row(o) + n_z) % n_z
+
+            def send(i, _):
+                s = (me.s8 + i) % SRC
+                remote(retb.at[o, s], reti.at[mine_e], ret_send, ret_sem, me.at(z, s)).start()
+                return 0
+
+            lax.fori_loop(1 if o == 0 else 0, SRC, send, 0)
+        if q == 0:
+            pltpu.make_async_copy(retb.at[0, me.s8], reti.at[mine_e], ret_sem).start()
+
+    for first in (0, 1):
+        send_far(first)
+        send_far(first + 2)
+        send_side(first + 2, True, False)
+        send_side(first, False, False)
+        send_side(first, True, True)
+        send_side(first + 2, False, True)
+    for q in (0, 2, 1, 3):
+        finish(q)
+
+    await_bytes(reti, ret_sem)
+    res = reti[...].reshape(64 * MSG, 3 * 128)
+    mixed = dot(wmix[0, 0], res) + dot(wmix[0, 1], res)
+    last = jnp.zeros((n_rows, 128), F32)
+    for j in range(3):
+        piece = res[:, 128 * j : 128 * (j + 1)]
+        last = last + dot(wmix[1 + j, 0], piece) + dot(wmix[1 + j, 1], piece)
+    fino[:, :, : 3 * 128] = mixed.astype(BF).reshape(4, quarter, 3 * 128)
+    fino[:, :, 3 * 128 :] = last.astype(BF).reshape(4, quarter, 128)
+    for step in (1, 2, 3):
+        remote(fino.at[(me.t + step) % 4], fini.at[step - 1], fin_send.at[step - 1], fin_sem.at[step - 1], me.x(step)).start()
+    out[:, mine] = fino[me.t]
+    for step in (1, 2, 3):
+        await_bytes(fini.at[step - 1], fin_sem.at[step - 1])
+        theirs = pl.ds(pl.multiple_of((me.t + 4 - step) % 4 * cols, cols), cols)
+        out[:, theirs] = fini[step - 1]
+
+    for step in (0, 1, 2):
+        await_bytes(fini.at[step], fin_send.at[step])
+    for q in range(4):
+        for k in range(3):
+            await_bytes(far.at[q], rs_send.at[k, q])
+    for b, k, n in ((0, 0, n_z), (0, 1, n_z), (1, 0, n_z // 2), (2, 1, n_z // 2)):
+        await_bytes(arr.at[b, pl.ds(0, n)], xs_sem.at[b, k])
+    for buf, sem in ((outb, out_sem), (retb, ret_send)):
+        await_bytes(buf.at[pl.ds(1, n_z - 1)], sem)
+        await_bytes(buf.at[0, pl.ds(1, SRC - 1)], sem)
+
+
 def experts_part(moe_tokens, moe_gain, routes, route_weights, w_gate, w_up, w_down):
-    n_rows = moe_tokens.shape[0]
-    model_dim = moe_tokens.shape[1]
-    top_count = routes.shape[1]
-    quarters = lax.axis_size("tp")
-    part_rows = n_rows // quarters
-    experts = lax.axis_size(EP) * w_gate.shape[0]
-    capacity = (3 * top_count * part_rows + 2 * experts - 1) // (2 * experts)
-    slot_count = experts * capacity
-    normed = rms_norm(moe_tokens.astype(jnp.float32), moe_gain).astype(jnp.bfloat16)
-    chosen = routes.reshape(quarters, part_rows * top_count)
-    onehot = (chosen[..., None] == jnp.arange(experts, dtype=jnp.int32)).astype(jnp.int32)
-    rank = jnp.sum((jnp.cumsum(onehot, axis=1) - onehot) * onehot, axis=-1)
-    slots = chosen * capacity + rank
-    slot_hit = (slots[..., None] == jnp.arange(slot_count, dtype=jnp.int32)).astype(jnp.bfloat16)
-    slot_hit = slot_hit.reshape(quarters, part_rows, top_count, slot_count)
-    my_part = lax.axis_index("tp")
-    mine_hit = lax.dynamic_index_in_dim(slot_hit, my_part, 0, keepdims=False)
-    down_cols = w_down[0]
-    own_rows = lax.dynamic_slice_in_dim(normed, my_part * part_rows, part_rows, 0)
-    outgoing = jnp.einsum(
-        "rs,rd->sd", jnp.sum(mine_hit, axis=1), own_rows, preferred_element_type=jnp.float32
-    )
-    outgoing = outgoing.astype(jnp.bfloat16).reshape(1, experts, capacity, model_dim)
-    arrived = lax.all_gather(
-        lax.all_to_all(outgoing, EP, split_axis=1, concat_axis=1, tiled=True),
-        "tp",
-        axis=0,
-        tiled=True,
-    )
-    gate = jnp.einsum("abcd,df->abcf", arrived, w_gate[0], preferred_element_type=jnp.float32)
-    upward = jnp.einsum("abcd,df->abcf", arrived, w_up[0], preferred_element_type=jnp.float32)
-    hidden = (jax.nn.silu(gate) * upward).astype(jnp.bfloat16)
-    summed = summed_on_arrival(
-        jnp.einsum("abcf,fd->abcd", hidden, down_cols, preferred_element_type=jnp.float32), "tp", 0
-    ).astype(jnp.bfloat16)
-    returned = core_and_chips(summed, (("ep_0", "ep_1"), "ep_2"), (0, 1), 1, 1)
-    picked = jnp.einsum(
-        "rks,sd->rkd",
-        mine_hit,
-        returned.reshape(slot_count, model_dim),
-        preferred_element_type=jnp.float32,
-    )
-    own_weights = lax.dynamic_slice_in_dim(route_weights, my_part * part_rows, part_rows, 0)
-    return jnp.sum(picked * own_weights[:, :, None], axis=1).astype(jnp.bfloat16)
+    n_z = lax.axis_size("ep_0")
+    n_rows, model = moe_tokens.shape
+    ff = w_gate.shape[2]
+    cols = model // 4
+    consts = fixed_selects()
+    vm = pl.BlockSpec(memory_space=pltpu.VMEM)
+    hbm = pl.BlockSpec(memory_space=pl.ANY)
+    chunk = (4, 192, cols)
+    dma = pltpu.SemaphoreType.DMA
+    slots = n_z * SRC * CAP
+    return pl.pallas_call(
+        functools.partial(experts_kernel, n_z),
+        out_shape=jax.ShapeDtypeStruct((n_rows // 4, model), BF),
+        in_specs=[vm] * 9 + [hbm] * 3,
+        out_specs=vm,
+        scratch_shapes=[
+            pltpu.VMEM((model, ff), BF),
+            pltpu.VMEM((model, ff), BF),
+            pltpu.VMEM((ff, model), BF),
+            pltpu.VMEM((n_rows, cols), BF),
+            pltpu.VMEM((n_z, SRC, MSG, 384), BF),
+            pltpu.VMEM((4, n_z, SRC, MSG, 384), BF),
+            pltpu.VMEM((4, slots, cols), BF),
+            pltpu.VMEM((slots, ff), F32),
+            pltpu.VMEM((slots, ff), F32),
+            pltpu.VMEM((slots, ff), BF),
+            pltpu.VMEM((4, 2, n_rows, 64 * MSG), BF),
+            pltpu.VMEM(chunk, BF),
+            pltpu.VMEM(chunk, BF),
+            pltpu.VMEM(chunk, BF),
+            pltpu.VMEM(chunk, BF),
+            pltpu.VMEM(chunk, BF),
+            pltpu.VMEM(chunk, BF),
+            pltpu.VMEM((n_z, SRC, MSG, 384), BF),
+            pltpu.VMEM((n_z * SRC, MSG, 384), BF),
+            pltpu.VMEM((4, n_rows // 4, cols), BF),
+            pltpu.VMEM((3, n_rows // 4, cols), BF),
+            dma((3,)),
+            dma((n_z,)),
+            dma,
+            dma,
+            dma((3, 2)),
+            dma((3, n_z)),
+            dma((3, 4)),
+            dma((4,)),
+            dma((4,)),
+            dma((4,)),
+            dma,
+            dma,
+            dma((3,)),
+            dma((3,)),
+        ],
+        compiler_params=pltpu.CompilerParams(collective_id=1, has_side_effects=True, vmem_limit_bytes=60 * 1024 * 1024),
+        name="experts",
+    )(
+        moe_tokens,
+        moe_gain.reshape(1, model),
+        routes,
+        routes.T,
+        route_weights,
+        *consts,
+        w_gate,
+        w_up,
+        w_down,
+    )
 
 
 def on_device(

time: 379 us -> 310 us (0.82)
  the two profiles are of different devices: /device:TPU:249 before, /device:TPU:251 now
where the time goes in v1:
time: 310 us; the launch traced here: 309 us
  Pallas kernels  109 us (35%)
  local copies, waits for them, and re-layouts  81.3 us (26%)
  matrix products  42.2 us (14%)
  waiting for transfers between devices  27.9 us (9%)
  loops' own time  24.2 us (8%)
  between operations  14.3 us (5%)
  other arithmetic  10.2 us (3%)
    pallas_call x1, Pallas kernels, experts_part(): pl.pallas_call(functools.partial(experts_kernel, n_z), out_shape=jax.Shap...  109 us
    slice x32, local copies, waits for them, and re-layouts, attend(): kv_block[:, :head_count * nope_dim]  42.8 us
    all_gather x1, waiting for transfers between devices, side_by_side(): whole = lax.all_gather(both, axis, axis=dim, tiled=True)  27.9 us
    another operation x1, loops' own time, attention_part(): lax.scan(one_block, totals, jnp.arange(piece_rows // block_rows, dtype=jn...  22.1 us
    dynamic_slice x32, local copies, waits for them, and re-layouts, attention_part(): lax.scan(one_block, totals, jnp.arange(piece_rows // block_rows, dtype=jn...  18.8 us
    dot_general x32, matrix products, attend(): jnp.einsum('qhr,kr->hqk', query_rope, rope_block, preferred_element_type=...  17 us
    split x2, local copies, waits for them, and re-layouts, side_by_side(): jnp.split(whole, [sum(widths[:k]) for k in range(1, len(widths))], axis=a...  15.5 us
    dot_general x32, matrix products, attend(): jnp.einsum('hqk,khd->qhd', exp_scores.astype(jnp.bfloat16), value_block,...  11.3 us
  transfers between devices with their start and end apart: 1, of which 1 were waited for; matrix products, arithmetic and copies ran while one was open for 1% of the time, Pallas kernels for 35%

profile of v1, /device:TPU:251, one launch (start us, length us, event | category | flops | bytes accessed | tf_op | source)
XLA Modules:
  0.0 309.1 jit_solution(14280080004391511594)
XLA Ops:
  11.2 1.4 convolution_convert_fusion
  17.5 108.9 %experts.1 = bf16[64,2048]{1,0:T(8,128)(2,1)} custom-call(bf16[256,2048]{1,0:T(8,128)(2,1)} %tokens.1, f32[1,2048]{1,0:T(1,128)} %bitcast.58, s32[256,2]{1,0:T(8,128)} %copy.36.routes, s32[2,256]{1,0:T(2,128)} %bitcast.59, f32[256,2]{1,0:T(8,128)} %copy.37.weights, bf16[192,256]{1,0:T(8,128)(2,1)} %constant.95.clone.un_main, ...), custom_call_target="tpu_custom_call" | custom-call | tf_op jit(solution)/shard_map/experts/pallas_call | solution.py:567
  126.5 27.9 %all-gather.2.cloned.1.call-done = bf16[16384,576]{0,1:T(8,128)(2,1)} async-done(((bf16[256,576]{0,1:T(8,128)(2,1)}), bf16[16384,576]{0,1:T(8,128)(2,1)}) %all-gather.2.cloned.1.call-update) | async-done | bytes 18874384 | tf_op jit(solution)/shard_map/all_gather | solution.py:27
  154.4 13.7 %split.8 = bf16[16384,512]{0,1:T(8,128)(2,1)} slice(bf16[16384,576]{0,1:T(8,128)(2,1)} %all-gather.2.cloned.1.call-done), slice={[0:16384], [0:512]} | slice | bytes 33554432 | tf_op jit(solution)/shard_map/split | solution.py:28
  168.2 1.7 split.9
  170.0 130.4 %while.13 = (s32[]{:T(128)}, f32[256,2,128]{2,0,1:T(8,128)S(1)}, f32[2,256]{1,0:T(2,128)S(1)}, s32[32]{0:T(128)S(1)}, s32[]{:T(128)}, /*index=5*/bf16[16384,512]...) while((s32[]{:T(128)}, f32[256,2,128]{2,0,1:T(8,128)S(1)}, ...), condition=%wide.region_8.9_spmd.clone, body=%wide.region_4.8_spmd.clone.sunk | while | flops 169280256 | bytes 5783885 | solution.py:174
  171.2 2.8 conditional.3
  171.3 1.3 constant_dynamic-slice_fusion
  175.3 2.8 conditional.3
  175.3 1.3 constant_dynamic-slice_fusion
  179.4 2.8 conditional.3
  183.5 2.8 conditional.3
  187.6 2.8 conditional.3
  191.6 2.8 conditional.3
  195.7 2.8 conditional.3
  195.7 1.3 constant_dynamic-slice_fusion
  199.8 2.8 conditional.3
  203.9 2.8 conditional.3
  203.9 1.3 constant_dynamic-slice_fusion
  207.9 2.8 conditional.3
  212.0 2.8 conditional.3
  212.0 1.3 constant_dynamic-slice_fusion
  216.1 2.8 conditional.3
  220.2 2.8 conditional.3
  220.2 1.3 constant_dynamic-slice_fusion
  224.2 2.8 conditional.3
  224.3 1.3 constant_dynamic-slice_fusion
  228.3 2.8 conditional.3
  228.3 1.3 constant_dynamic-slice_fusion
  232.4 2.8 conditional.3
  232.4 1.3 constant_dynamic-slice_fusion
  236.5 2.8 conditional.3
  236.5 1.3 constant_dynamic-slice_fusion
  240.5 2.8 conditional.3
  244.6 2.8 conditional.3
  248.7 2.8 conditional.3
  252.8 2.8 conditional.3
  256.8 2.8 conditional.3
  260.9 2.8 conditional.3
  265.0 2.8 conditional.3
  269.1 2.8 conditional.3
  273.1 2.8 conditional.3
  277.2 2.8 conditional.3
  281.3 2.8 conditional.3
  285.4 2.8 conditional.3
  289.4 2.8 conditional.3
  293.5 2.8 conditional.3
  297.6 2.8 conditional.3
  (354 shorter events, 103.5 us)
Async XLA Ops:
  7.2 2.0 copy-start
  7.2 8.5 %copy-start.4 = (f32[192]{0:T(256)S(1)}, f32[192]{0:T(256)}, u32[]{:S(2)}) copy-start(f32[192]{0:T(256)} %param.31) | copy-start | bytes 2308
  7.2 8.7 %copy-start.2 = (s32[256,2]{0,1:T(2,128)S(1)}, s32[256,2]{0,1:T(2,128)}, u32[]{:S(2)}) copy-start(s32[256,2]{0,1:T(2,128)} %param.37) | copy-start | bytes 6148
  7.2 9.5 %copy-start.3 = (f32[256,2]{0,1:T(2,128)S(1)}, f32[256,2]{0,1:T(2,128)}, u32[]{:S(2)}) copy-start(f32[256,2]{0,1:T(2,128)} %param.38) | copy-start | bytes 6148
  7.2 147.2 %all-gather.2.cloned.1.call-start = ((), (), s32[]{:S(2)}) async-start(), calls=%async_computation | async-start | bytes 19169280 | tf_op jit(solution)/shard_map/all_gather | solution.py:27
  170.0 130.7 %copy-start.5 = (f32[128]{0:T(128)S(1)}, f32[128]{0:T(128)}, u32[]{:S(2)}) copy-start(f32[128]{0:T(128)} %param.34) | copy-start | bytes 1540
  170.0 131.5 %copy-start.1 = (bf16[64,2048]{1,0:T(8,128)(2,1)S(1)}, bf16[64,2048]{1,0:T(8,128)(2,1)}, u32[]{:S(2)}) copy-start(bf16[64,2048]{1,0:T(8,128)(2,1)} %experts.1) | copy-start | bytes 786436
Sparse Core Ops, SparseCore 0:
  14.6 139.7 all-gather.1

commit v2 on v1

--- a/solution.py
+++ b/solution.py
@@ -21,160 +21,10 @@
 THETA = 500000.0
 
 
-def side_by_side(arrays, axis, dim, along):
-    widths = [a.shape[along] for a in arrays]
-    both = jnp.concatenate(arrays, axis=along)
-    whole = lax.all_gather(both, axis, axis=dim, tiled=True)
-    return tuple(jnp.split(whole, [sum(widths[:k]) for k in range(1, len(widths))], axis=along))
-
-
-def in_blocks(x, dim, count):
-    dims = x.shape
-    blocks = x.reshape(*dims[:dim], count, dims[dim] // count, *dims[dim + 1 :])
-    return jnp.moveaxis(blocks, dim, 0)
-
-
-def summed_on_arrival(x, axis, dim):
-    count = lax.axis_size(axis)
-    blocks = lax.all_to_all(in_blocks(x, dim, count), axis, 0, 0, tiled=True)
-    return jnp.sum(blocks, axis=0)
-
-
-def joined_along(blocks, dim):
-    blocks = jnp.moveaxis(blocks, 0, dim)
-    dims = blocks.shape
-    return blocks.reshape(*dims[:dim], dims[dim] * dims[dim + 1], *dims[dim + 2 :])
-
-
-def moved_by_axis(blocks, axes, order):
-    dims = [lax.axis_size(a) for a in axes]
-    blocks = blocks.reshape(*dims, *blocks.shape[1:])
-    for k in order:
-        blocks = lax.all_to_all(blocks, axes[k], split_axis=k, concat_axis=k, tiled=True)
-    return blocks.reshape(-1, *blocks.shape[len(axes) :])
-
-
-def core_and_chips(x, groups, order, split_dim, concat_dim):
-    count = lax.axis_size(groups[0]) * lax.axis_size(groups[1])
-    blocks = in_blocks(x, split_dim, count)
-    return joined_along(moved_by_axis(blocks, groups, order), concat_dim)
-
-
-def rms_norm(values, norm_gain):
-    return values * lax.rsqrt(jnp.mean(values * values, axis=-1, keepdims=True) + EPS) * norm_gain
-
-
 def rope_tables(positions, rope_dim):
     freqs = 1.0 / THETA ** (jnp.arange(0, rope_dim, 2, dtype=jnp.float32) / rope_dim)
     angles = positions.astype(jnp.float32)[:, None] * freqs[None, :]
     return (jnp.cos(angles), jnp.sin(angles))
-
-
-def rotate(values, rot_cos, rot_sin):
-    half_dim = values.shape[-1] // 2
-    first_half = values[..., :half_dim]
-    second_half = values[..., half_dim:]
-    return jnp.concatenate(
-        [
-            first_half * rot_cos - second_half * rot_sin,
-            second_half * rot_cos + first_half * rot_sin,
-        ],
-        axis=-1,
-    )
-
-
-def attention_part(
-    queries,
-    kv_latent,
-    rope_key,
-    latent_gain,
-    w_key_up,
-    w_value_up,
-    query_gain,
-    key_gain,
-    rope_gain,
-    out_gain,
-):
-    tok_rows = queries.shape[0]
-    nope_dim = key_gain.shape[0]
-    value_dim = out_gain.shape[0]
-    rope_dim = rope_key.shape[1]
-    head_count = w_key_up.shape[1] // nope_dim
-    offset = lax.axis_index(EP) * tok_rows
-    positions = offset + jnp.arange(tok_rows, dtype=jnp.int32)
-    rot_cos, rot_sin = rope_tables(positions, rope_dim)
-    latent = rms_norm(kv_latent.astype(jnp.float32), latent_gain).astype(jnp.bfloat16)
-    key_nope = jnp.dot(latent, w_key_up, preferred_element_type=jnp.float32).reshape(
-        tok_rows, head_count, nope_dim
-    )
-    key_nope = (
-        rms_norm(key_nope, key_gain).astype(jnp.bfloat16).reshape(tok_rows, head_count * nope_dim)
-    )
-    values = jnp.dot(latent, w_value_up, preferred_element_type=jnp.float32).astype(jnp.bfloat16)
-    rot_key = rotate(rms_norm(rope_key.astype(jnp.float32), rope_gain), rot_cos, rot_sin).astype(
-        jnp.bfloat16
-    )
-    keys_values = jnp.concatenate([key_nope, values], axis=1)
-    query = rms_norm(
-        queries.astype(jnp.float32).reshape(tok_rows, head_count, nope_dim + rope_dim), query_gain
-    )
-    query_nope = query[..., :nope_dim].astype(jnp.bfloat16)
-    query_rope = rotate(query[..., nope_dim:], rot_cos[:, None, :], rot_sin[:, None, :]).astype(
-        jnp.bfloat16
-    )
-    scale = (nope_dim + rope_dim) ** (-0.5)
-    last_pos = offset + tok_rows - 1
-    initial = (
-        jnp.zeros((tok_rows, head_count, value_dim), jnp.float32),
-        jnp.zeros((head_count, tok_rows), jnp.float32),
-    )
-    totals = initial
-    key_piece, rope_piece = side_by_side((keys_values, rot_key), EP, 0, 1)
-    piece_rows = key_piece.shape[0]
-    block_rows = math.gcd(piece_rows, 512)
-
-    def one_block(totals_in, block_index):
-        block_first = block_index * block_rows
-        kv_block = lax.dynamic_slice_in_dim(key_piece, block_first, block_rows, 0)
-        rope_block = lax.dynamic_slice_in_dim(rope_piece, block_first, block_rows, 0)
-
-        def attend(sums_in):
-            weighted, denominator = sums_in
-            key_block = kv_block[:, : head_count * nope_dim].reshape(
-                block_rows, head_count, nope_dim
-            )
-            value_block = kv_block[:, head_count * nope_dim :].reshape(
-                block_rows, head_count, value_dim
-            )
-            scores = (
-                jnp.einsum(
-                    "qhd,khd->hqk", query_nope, key_block, preferred_element_type=jnp.float32
-                )
-                + jnp.einsum(
-                    "qhr,kr->hqk", query_rope, rope_block, preferred_element_type=jnp.float32
-                )
-            ) * scale
-            key_pos = block_first + jnp.arange(block_rows, dtype=jnp.int32)
-            visible = (positions[:, None] >= key_pos[None, :])[None]
-            exp_scores = jnp.where(visible, jnp.exp(scores), 0.0)
-            denominator = denominator + jnp.sum(exp_scores, axis=-1)
-            weighted = weighted + jnp.einsum(
-                "hqk,khd->qhd",
-                exp_scores.astype(jnp.bfloat16),
-                value_block,
-                preferred_element_type=jnp.float32,
-            )
-            return (weighted, denominator)
-
-        def unchanged(sums_in):
-            return sums_in
-
-        return (lax.cond(block_first <= last_pos, attend, unchanged, totals_in), None)
-
-    totals, _ = lax.scan(one_block, totals, jnp.arange(piece_rows // block_rows, dtype=jnp.int32))
-    weighted, denominator = totals
-    mixed = weighted / jnp.transpose(denominator)[:, :, None]
-    return rms_norm(mixed, out_gain).astype(jnp.bfloat16).reshape(tok_rows, head_count * value_dim)
 
 
 SRC = 8
@@ -621,6 +471,320 @@
     )
 
 
+HEAD = 128
+ROPE = 64
+UP, DOWN = 4, 3
+
+
+class Attention:
+    def __init__(self, n_z, me, ins, out, buf, sem):
+        self.n_z, self.me, self.ins, self.out, self.buf, self.sem = n_z, me, ins, out, buf, sem
+
+    def prepare(self):
+        me = self.me
+        (queries, kv_latent, rope2, lat_gain, wk, wv, qn_gain, qr_gain, key_gain, rope_gain, _, cos2, sin2) = self.ins
+        kv, rk, kvb, rkb, q_all, qb = (self.buf[k] for k in ("kv", "rk", "kvb", "rkb", "q_all", "qb"))
+        n = queries.shape[0]
+        lane = lax.broadcasted_iota(I32, (n, 128), 1)
+        low = lane < ROPE
+
+        def turned(v):
+            other = jnp.where(lane % ROPE < ROPE // 2, pltpu.roll(v, 128 - ROPE // 2, 1), pltpu.roll(v, ROPE // 2, 1))
+            return v * cos2[...] + other * sin2[...]
+
+        v = kv_latent[...].astype(F32)
+        latent = (v * lax.rsqrt(jnp.mean(v * v, axis=-1, keepdims=True) + EPS) * lat_gain[...]).astype(BF)
+        keys = dot(latent, wk[...])
+        vals = dot(latent, wv[...]).astype(BF)
+        for h in (0, 1):
+            k = keys[:, HEAD * h : HEAD * (h + 1)]
+            k = k * lax.rsqrt(jnp.mean(k * k, axis=-1, keepdims=True) + EPS) * key_gain[...]
+            kvb[h, :, :HEAD] = k.astype(BF)
+            kvb[h, :, HEAD:] = vals[:, HEAD * h : HEAD * (h + 1)]
+        r = rope2[...].astype(F32)
+        r = turned(r * lax.rsqrt(jnp.mean(r * r, axis=-1, keepdims=True) + EPS) * rope_gain[...])
+        rkb[...] = jnp.where(low[: n // 2], r[: n // 2], r[n // 2 :]).astype(BF)
+
+        t0, t1, t2 = (queries[:, 128 * j : 128 * (j + 1)].astype(F32) for j in range(3))
+        total = lambda a: jnp.sum(a, axis=-1, keepdims=True)
+        s1 = t1 * t1
+        width = HEAD + ROPE
+        inv0 = lax.rsqrt((total(t0 * t0) + total(jnp.where(low, s1, 0.0))) / width + EPS)
+        inv1 = lax.rsqrt((total(t2 * t2) + total(jnp.where(low, 0.0, s1))) / width + EPS)
+        nope1 = jnp.where(low, pltpu.roll(t1, ROPE, 1), pltpu.roll(t2, ROPE, 1))
+        turn = turned(jnp.where(low, t1 * inv0, t2 * inv1) * qr_gain[...])
+        qb[0, :, :HEAD] = (t0 * inv0 * qn_gain[...]).astype(BF)
+        qb[1, :, :HEAD] = (nope1 * inv1 * qn_gain[...]).astype(BF)
+        qb[0, :, HEAD:] = jnp.where(low, turn, 0.0).astype(BF)
+        qb[1, :, HEAD:] = jnp.where(low, 0.0, turn).astype(BF)
+        q_all[me.s8] = qb[me.c]
+        kv[0, self.mine(256)] = kvb[me.c]
+        rk[0, self.mine(128)] = rkb[...]
+
+    def mine(self, n):
+        return pl.ds(pl.multiple_of(self.me.c * n, n), n)
+
+    def send_first(self):
+        me, b, s = self.me, self.buf, self.sem
+        other = (me.z, me.y, 1 - me.c, me.t)
+        remote(b["kvb"].at[1 - me.c], b["kv"].at[0, self.mine(256)], s["kv_out"].at[0], s["kv_in"].at[0], other).start()
+        remote(b["rkb"], b["rk"].at[0, self.mine(128)], s["kv_out"].at[1], s["rk_in"].at[0], other).start()
+
+        def one(i, _):
+            d = (me.s8 + i) % SRC
+            remote(b["qb"].at[d % 2], b["q_all"].at[me.s8], s["q_out"], s["q_in"], me.at(me.z, d)).start()
+            return 0
+
+        lax.fori_loop(1, SRC, one, 0)
+
+    def first_in(self):
+        b, s = self.buf, self.sem
+        await_bytes(b["kvb"].at[0], s["kv_in"].at[0])
+        await_bytes(b["rkb"], s["rk_in"].at[0])
+
+    def queries_in(self):
+        await_bytes(self.buf["q_all"].at[pl.ds(0, SRC - 1)], self.sem["q_in"])
+
+    def has(self, slot):
+        z = self.me.z
+        if slot <= UP:
+            return z >= slot
+        return (z + slot - UP) % self.n_z < DOWN
+
+    def uses(self, slot):
+        z = self.me.z
+        return z >= slot if slot <= UP else z + slot - UP >= self.n_z
+
+    def sends(self, slot, up):
+        z = self.me.z
+        if up:
+            return (z <= self.n_z - 2) & (z >= slot)
+        back = 0 if slot == 0 else slot - UP
+        return (z + back) % self.n_z < DOWN
+
+    def _copies(self, slot, up):
+        me, b, s = self.me, self.buf, self.sem
+        to = slot + 1 if up else (UP + 1 if slot == 0 else slot + 1)
+        z = (me.z + (1 if up else self.n_z - 1)) % self.n_z
+        where = (z, me.y, me.c, me.t)
+        return (
+            remote(b["kv"].at[slot], b["kv"].at[to], s["hop_out"].at[to, 0], s["kv_in"].at[to], where),
+            remote(b["rk"].at[slot], b["rk"].at[to], s["hop_out"].at[to, 1], s["rk_in"].at[to], where),
+        )
+
+    def hop(self, slot, up):
+        @pl.when(self.sends(slot, up))
+        def _():
+            for copy in self._copies(slot, up):
+                copy.start()
+
+    def arrive(self, slot):
+        b, s = self.buf, self.sem
+
+        @pl.when(self.has(slot))
+        def _():
+            await_bytes(b["kv"].at[slot], s["kv_in"].at[slot])
+            await_bytes(b["rk"].at[slot], s["rk_in"].at[slot])
+
+        if slot < UP:
+            self.hop(slot, True)
+        elif UP < slot < UP + DOWN:
+            self.hop(slot, False)
+
+    def attend(self, slot):
+        @pl.when(self.uses(slot))
+        def _():
+            self._attend(slot)
+
+    def _attend(self, slot):
+        me = self.me
+        kv, rk, q_all, acc, kop, vop = (self.buf[k] for k in ("kv", "rk", "q_all", "acc", "kop", "vop"))
+        n_keys = kv.shape[1]
+        packed = rk[slot].astype(F32)
+        rolled = pltpu.roll(packed, ROPE, 1)
+        low = lax.broadcasted_iota(I32, packed.shape, 1) < ROPE
+        lo = jnp.where(low, packed, rolled).astype(BF)
+        hi = jnp.where(low, rolled, packed).astype(BF)
+        kop[:, :HEAD] = kv[slot, :, :HEAD]
+        for half in (0, 1):
+            kop[256 * half : 256 * half + 128, HEAD:] = lo[128 * half : 128 * half + 128]
+            kop[256 * half + 128 : 256 * half + 256, HEAD:] = hi[128 * half : 128 * half + 128]
+        vop[:, :HEAD] = kv[slot, :, HEAD:]
+        scale = (HEAD + ROPE) ** (-0.5) * math.log2(math.e)
+        per = 512
+
+        def one(m, _):
+            q = q_all[pl.ds(2 * m, 2)].reshape(per, 2 * HEAD)
+            s = lax.dot_general(q, kop[...], (((1,), (1,)), ((), ())), preferred_element_type=F32)
+            e = jnp.exp2(s * scale)
+            if slot == 0:
+                at_q = lax.broadcasted_iota(I32, (per, n_keys), 0) + m * per
+                at_k = lax.broadcasted_iota(I32, (per, n_keys), 1) + me.y * n_keys
+                e = jnp.where(at_q >= at_k, e, 0.0)
+            got = dot(e.astype(BF), vop[...]).reshape(2, 256, 2 * HEAD)
+            if slot == 0:
+                acc[pl.ds(2 * m, 2)] = got
+            else:
+                acc[pl.ds(2 * m, 2)] += got
+            return 0
+
+        lax.fori_loop(0, SRC * 256 // per, one, 0)
+
+    def ones(self):
+        vop = self.buf["vop"]
+        vop[:, HEAD:] = jnp.ones((vop.shape[0], HEAD), BF)
+
+    def send_sums(self):
+        me, b, s = self.me, self.buf, self.sem
+        acc, ob, db, od, dd = (b[k] for k in ("acc", "ob", "db", "od", "dd"))
+
+        def halves(m):
+            a = acc[m]
+            return a[:, :HEAD].astype(BF), jnp.transpose(a[:, HEAD:])[:8]
+
+        def one(i, _):
+            m = (me.s8 + i) % SRC
+            ob[m], db[m] = halves(m)
+            where = me.at(me.z, m)
+            remote(ob.at[m], od.at[me.s8], s["o_out"].at[0], s["o_in"].at[0], where).start()
+            remote(db.at[m], dd.at[me.s8], s["o_out"].at[1], s["o_in"].at[1], where).start()
+            return 0
+
+        lax.fori_loop(1, SRC, one, 0)
+        od[me.s8], dd[me.s8] = halves(me.s8)
+
+    def finish(self):
+        b, s = self.buf, self.sem
+        od, dd = b["od"], b["dd"]
+        out_gain = self.ins[10]
+        await_bytes(od.at[pl.ds(0, SRC - 1)], s["o_in"].at[0])
+        await_bytes(dd.at[pl.ds(0, SRC - 1)], s["o_in"].at[1])
+        for h in (0, 1):
+            o = sum(od[2 * y + h].astype(F32) for y in range(4))
+            d = sum(dd[2 * y + h] for y in range(4))
+            den = jnp.transpose(jnp.broadcast_to(d[0:1], (HEAD, d.shape[1])))
+            m = o / den
+            m = m * lax.rsqrt(jnp.mean(m * m, axis=-1, keepdims=True) + EPS) * out_gain[...]
+            self.out[:, HEAD * h : HEAD * (h + 1)] = m.astype(BF)
+
+    def drain(self):
+        b, s = self.buf, self.sem
+        await_bytes(b["kvb"].at[0], s["kv_out"].at[0])
+        await_bytes(b["rkb"], s["kv_out"].at[1])
+        await_bytes(b["q_all"].at[pl.ds(0, SRC - 1)], s["q_out"])
+        for slot, up in [(k, True) for k in range(UP)] + [(0, False)] + [(UP + k, False) for k in range(1, DOWN)]:
+
+            @pl.when(self.sends(slot, up))
+            def _():
+                for copy in self._copies(slot, up):
+                    copy.wait_send()
+
+        await_bytes(b["od"].at[pl.ds(0, SRC - 1)], s["o_out"].at[0])
+        await_bytes(b["dd"].at[pl.ds(0, SRC - 1)], s["o_out"].at[1])
+
+
+ATT_BUFS = {
+    "kv": ((8, 512, 256), "bf"),
+    "rk": ((8, 256, 128), "bf"),
+    "kvb": ((2, 256, 256), "bf"),
+    "rkb": ((128, 128), "bf"),
+    "q_all": ((8, 256, 256), "bf"),
+    "qb": ((2, 256, 256), "bf"),
+    "acc": ((8, 256, 256), "f"),
+    "kop": ((512, 256), "bf"),
+    "vop": ((512, 256), "bf"),
+    "ob": ((8, 256, 128), "bf"),
+    "db": ((8, 8, 256), "f"),
+    "od": ((8, 256, 128), "bf"),
+    "dd": ((8, 8, 256), "f"),
+}
+ATT_SEMS = {"kv_out": (2,), "kv_in": (8,), "rk_in": (8,), "q_out": None, "q_in": None, "hop_out": (8, 2), "o_out": (2,), "o_in": (2,)}
+
+
+def att_scratch():
+    bufs = [pltpu.VMEM(shape, BF if kind == "bf" else F32) for shape, kind in ATT_BUFS.values()]
+    sems = [pltpu.SemaphoreType.DMA if n is None else pltpu.SemaphoreType.DMA(n) for n in ATT_SEMS.values()]
+    return bufs + sems
+
+
+def att_refs(refs):
+    n = len(ATT_BUFS)
+    return dict(zip(ATT_BUFS, refs[:n])), dict(zip(ATT_SEMS, refs[n:]))
+
+
+def att_inputs(queries, kv_latent, rope_key, latent_gain, w_key_up, w_value_up, query_gain, key_gain, rope_gain, out_gain):
+    n = queries.shape[0]
+    positions = lax.axis_index(EP) * n + jnp.arange(n, dtype=I32)
+    cos, sin = rope_tables(positions, ROPE)
+    row = lambda g: g.reshape(1, -1)
+    twice = lambda g: jnp.concatenate([g, g], axis=-1)
+    return (
+        queries,
+        kv_latent,
+        twice(rope_key),
+        row(latent_gain),
+        w_key_up,
+        w_value_up,
+        row(query_gain[:HEAD]),
+        row(twice(query_gain[HEAD:])),
+        row(key_gain),
+        row(twice(rope_gain)),
+        row(out_gain),
+        twice(twice(cos)),
+        twice(jnp.concatenate([-sin, sin], axis=-1)),
+    )
+
+
+def attention_kernel(n_z, *refs):
+    ins, out, rest = refs[:13], refs[13], refs[14:]
+    me = Place(n_z)
+    buf, sem = att_refs(rest)
+    barrier = pltpu.get_barrier_semaphore()
+
+    def one(i, _):
+        pl.semaphore_signal(barrier, inc=1, device_id=me.at(me.z, (me.s8 + i) % SRC), device_id_type=MESH)
+        return 0
+
+    lax.fori_loop(1, SRC, one, 0)
+    for step in (1, n_z - 1):
+        pl.semaphore_signal(barrier, inc=1, device_id=((me.z + step) % n_z, me.y, me.c, me.t), device_id_type=MESH)
+    att = Attention(n_z, me, ins, out, buf, sem)
+    att.prepare()
+    att.ones()
+    pl.semaphore_wait(barrier, SRC - 1 + 2)
+    att.send_first()
+    att.first_in()
+    att.hop(0, True)
+    att.hop(0, False)
+    att.queries_in()
+    att.attend(0)
+    for k in range(1, UP + 1):
+        att.arrive(k)
+        if k <= DOWN:
+            att.arrive(UP + k)
+        att.attend(k)
+        if k <= DOWN:
+            att.attend(UP + k)
+    att.send_sums()
+    att.finish()
+    att.drain()
+
+
+def attention_part(*args):
+    n_z = lax.axis_size("ep_0")
+    ins = att_inputs(*args)
+    vm = pl.BlockSpec(memory_space=pltpu.VMEM)
+    return pl.pallas_call(
+        functools.partial(attention_kernel, n_z),
+        out_shape=jax.ShapeDtypeStruct((256, 256), BF),
+        in_specs=[vm] * 13,
+        out_specs=vm,
+        scratch_shapes=att_scratch(),
+        compiler_params=pltpu.CompilerParams(collective_id=2, has_side_effects=True, vmem_limit_bytes=60 * 1024 * 1024),
+        name="attention",
+    )(*ins)
+
+
 def on_device(
     queries,
     kv_latent,

time: 310 us -> 177 us (0.57)
  the two profiles are of different devices: /device:TPU:251 before, /device:TPU:1 now
where the time goes in v2:
time: 177 us; the launch traced here: 176 us
  Pallas kernels  164 us (93%)
  local copies, waits for them, and re-layouts  8.02 us (5%)
  other arithmetic  3.63 us (2%)
    pallas_call x1, Pallas kernels, experts_part(): pl.pallas_call(functools.partial(experts_kernel, n_z), out_shape=jax.Shap...  124 us
    pallas_call x1, Pallas kernels, attention_part(): pl.pallas_call(functools.partial(attention_kernel, n_z), out_shape=jax.Sh...  40 us
    unnamed x7, local copies, waits for them, and re-layouts  6.15 us

profile of v2, /device:TPU:1, one launch (start us, length us, event | category | flops | bytes accessed | tf_op | source)
XLA Modules:
  0.0 176.3 jit_solution(5354262771175106317)
XLA Ops:
  0.7 0.5 fusion
  1.2 1.0 pad_maximum_fusion
  2.2 0.7 slice.7
  2.9 1.4 maximum_bitcast_fusion
  4.2 0.9 copy.27
  5.1 0.7 pad_maximum_fusion.2.refs_2_
  5.8 1.2 slice_bitcast_fusion.refs_6_
  7.0 40.0 %attention.1 = bf16[256,256]{1,0:T(8,128)(2,1)} custom-call(bf16[256,384]{1,0:T(8,128)(2,1)} %refs_0_.1, bf16[256,512]{1,0:T(8,128)(2,1)} %refs_1_.1, bf16[256,128]{1,0:T(8,128)(2,1)} %pad_maximum_fusion.2.refs_2_, f32[1,512]{1,0:T(1,128)} %bitcast.13, bf16[512,256]{1,0:T(8,128)(2,1)} %refs_4_.1, bf16[512,256]{1,0:T(8,128)(2,1)} %refs_5_.1, ...), custom_call_target="tpu_custom_call" | custom-call | tf_op jit(solution)/shard_map/attention/pallas_call | solution.py:777
  47.0 1.5 copy.30.routes
  48.5 1.5 copy.31.weights
  50.0 0.0 copy-start
  50.0 124.0 %experts.1 = bf16[64,2048]{1,0:T(8,128)(2,1)} custom-call(bf16[256,2048]{1,0:T(8,128)(2,1)} %tokens.1, f32[1,2048]{1,0:T(1,128)} %bitcast.11, s32[256,2]{1,0:T(8,128)} %copy.30.routes, s32[2,256]{1,0:T(2,128)} %bitcast.12, f32[256,2]{1,0:T(8,128)} %copy.31.weights, bf16[192,256]{1,0:T(8,128)(2,1)} %constant.37.clone.un_main, ...), custom_call_target="tpu_custom_call" | custom-call | tf_op jit(solution)/shard_map/experts/pallas_call | solution.py:417
  174.0 0.0 copy-done
  174.0 0.7 copy.34
  174.6 1.7 copy.35
  (2 shorter events, 0.0 us)
Async XLA Ops:
  50.0 124.0 %copy-start = (bf16[256,256]{1,0:T(8,128)(2,1)S(1)}, bf16[256,256]{1,0:T(8,128)(2,1)}, u32[]{:S(2)}) copy-start(bf16[256,256]{1,0:T(8,128)(2,1)} %attention.1) | copy-start | bytes 393220

commit v3 on v1

--- a/solution.py
+++ b/solution.py
@@ -19,162 +19,6 @@
 
 EPS = 1e-06
 THETA = 500000.0
-
-
-def side_by_side(arrays, axis, dim, along):
-    widths = [a.shape[along] for a in arrays]
-    both = jnp.concatenate(arrays, axis=along)
-    whole = lax.all_gather(both, axis, axis=dim, tiled=True)
-    return tuple(jnp.split(whole, [sum(widths[:k]) for k in range(1, len(widths))], axis=along))
-
-
-def in_blocks(x, dim, count):
-    dims = x.shape
-    blocks = x.reshape(*dims[:dim], count, dims[dim] // count, *dims[dim + 1 :])
-    return jnp.moveaxis(blocks, dim, 0)
-
-
-def summed_on_arrival(x, axis, dim):
-    count = lax.axis_size(axis)
-    blocks = lax.all_to_all(in_blocks(x, dim, count), axis, 0, 0, tiled=True)
-    return jnp.sum(blocks, axis=0)
-
-
-def joined_along(blocks, dim):
-    blocks = jnp.moveaxis(blocks, 0, dim)
-    dims = blocks.shape
-    return blocks.reshape(*dims[:dim], dims[dim] * dims[dim + 1], *dims[dim + 2 :])
-
-
-def moved_by_axis(blocks, axes, order):
-    dims = [lax.axis_size(a) for a in axes]
-    blocks = blocks.reshape(*dims, *blocks.shape[1:])
-    for k in order:
-        blocks = lax.all_to_all(blocks, axes[k], split_axis=k, concat_axis=k, tiled=True)
-    return blocks.reshape(-1, *blocks.shape[len(axes) :])
-
-
-def core_and_chips(x, groups, order, split_dim, concat_dim):
-    count = lax.axis_size(groups[0]) * lax.axis_size(groups[1])
-    blocks = in_blocks(x, split_dim, count)
-    return joined_along(moved_by_axis(blocks, groups, order), concat_dim)
-
-
-def rms_norm(values, norm_gain):
-    return values * lax.rsqrt(jnp.mean(values * values, axis=-1, keepdims=True) + EPS) * norm_gain
-
-
-def rope_tables(positions, rope_dim):
-    freqs = 1.0 / THETA ** (jnp.arange(0, rope_dim, 2, dtype=jnp.float32) / rope_dim)
-    angles = positions.astype(jnp.float32)[:, None] * freqs[None, :]
-    return (jnp.cos(angles), jnp.sin(angles))
-
-
-def rotate(values, rot_cos, rot_sin):
-    half_dim = values.shape[-1] // 2
-    first_half = values[..., :half_dim]
-    second_half = values[..., half_dim:]
-    return jnp.concatenate(
-        [
-            first_half * rot_cos - second_half * rot_sin,
-            second_half * rot_cos + first_half * rot_sin,
-        ],
-        axis=-1,
-    )
-
-
-def attention_part(
-    queries,
-    kv_latent,
-    rope_key,
-    latent_gain,
-    w_key_up,
-    w_value_up,
-    query_gain,
-    key_gain,
-    rope_gain,
-    out_gain,
-):
-    tok_rows = queries.shape[0]
-    nope_dim = key_gain.shape[0]
-    value_dim = out_gain.shape[0]
-    rope_dim = rope_key.shape[1]
-    head_count = w_key_up.shape[1] // nope_dim
-    offset = lax.axis_index(EP) * tok_rows
-    positions = offset + jnp.arange(tok_rows, dtype=jnp.int32)
-    rot_cos, rot_sin = rope_tables(positions, rope_dim)
-    latent = rms_norm(kv_latent.astype(jnp.float32), latent_gain).astype(jnp.bfloat16)
-    key_nope = jnp.dot(latent, w_key_up, preferred_element_type=jnp.float32).reshape(
-        tok_rows, head_count, nope_dim
-    )
-    key_nope = (
-        rms_norm(key_nope, key_gain).astype(jnp.bfloat16).reshape(tok_rows, head_count * nope_dim)
-    )
-    values = jnp.dot(latent, w_value_up, preferred_element_type=jnp.float32).astype(jnp.bfloat16)
-    rot_key = rotate(rms_norm(rope_key.astype(jnp.float32), rope_gain), rot_cos, rot_sin).astype(
-        jnp.bfloat16
-    )
-    keys_values = jnp.concatenate([key_nope, values], axis=1)
-    query = rms_norm(
-        queries.astype(jnp.float32).reshape(tok_rows, head_count, nope_dim + rope_dim), query_gain
-    )
-    query_nope = query[..., :nope_dim].astype(jnp.bfloat16)
-    query_rope = rotate(query[..., nope_dim:], rot_cos[:, None, :], rot_sin[:, None, :]).astype(
-        jnp.bfloat16
-    )
-    scale = (nope_dim + rope_dim) ** (-0.5)
-    last_pos = offset + tok_rows - 1
-    initial = (
-        jnp.zeros((tok_rows, head_count, value_dim), jnp.float32),
-        jnp.zeros((head_count, tok_rows), jnp.float32),
-    )
-    totals = initial
-    key_piece, rope_piece = side_by_side((keys_values, rot_key), EP, 0, 1)
-    piece_rows = key_piece.shape[0]
-    block_rows = math.gcd(piece_rows, 512)
-
-    def one_block(totals_in, block_index):
-        block_first = block_index * block_rows
-        kv_block = lax.dynamic_slice_in_dim(key_piece, block_first, block_rows, 0)
-        rope_block = lax.dynamic_slice_in_dim(rope_piece, block_first, block_rows, 0)
-
-        def attend(sums_in):
-            weighted, denominator = sums_in
-            key_block = kv_block[:, : head_count * nope_dim].reshape(
-                block_rows, head_count, nope_dim
-            )
-            value_block = kv_block[:, head_count * nope_dim :].reshape(
-                block_rows, head_count, value_dim
-            )
-            scores = (
-                jnp.einsum(
-                    "qhd,khd->hqk", query_nope, key_block, preferred_element_type=jnp.float32
-                )
-                + jnp.einsum(
-                    "qhr,kr->hqk", query_rope, rope_block, preferred_element_type=jnp.float32
-                )
-            ) * scale
-            key_pos = block_first + jnp.arange(block_rows, dtype=jnp.int32)
-            visible = (positions[:, None] >= key_pos[None, :])[None]
-            exp_scores = jnp.where(visible, jnp.exp(scores), 0.0)
-            denominator = denominator + jnp.sum(exp_scores, axis=-1)
-            weighted = weighted + jnp.einsum(
-                "hqk,khd->qhd",
-                exp_scores.astype(jnp.bfloat16),
-                value_block,
-                preferred_element_type=jnp.float32,
-            )
-            return (weighted, denominator)
-
-        def unchanged(sums_in):
-            return sums_in
-
-        return (lax.cond(block_first <= last_pos, attend, unchanged, totals_in), None)
-
-    totals, _ = lax.scan(one_block, totals, jnp.arange(piece_rows // block_rows, dtype=jnp.int32))
-    weighted, denominator = totals
-    mixed = weighted / jnp.transpose(denominator)[:, :, None]
-    return rms_norm(mixed, out_gain).astype(jnp.bfloat16).reshape(tok_rows, head_count * value_dim)
 
 
 SRC = 8
@@ -249,58 +93,310 @@
     return jnp.dot(a, b, preferred_element_type=F32)
 
 
-def experts_kernel(
-    n_z,
-    tokens,
-    gain,
-    routes,
-    routes_t,
-    weights,
-    un_main,
-    un_extra,
-    pk_main,
-    pk_extra,
-    wg_hbm,
-    wu_hbm,
-    wd_hbm,
-    out,
-    wg,
-    wu,
-    wd,
-    normed,
-    outb,
-    arr,
-    rows,
-    gacc,
-    uacc,
-    hid,
-    wmix,
-    far,
-    to_r,
-    to_l,
-    relay,
-    from_l,
-    from_r,
-    retb,
-    reti,
-    fino,
-    fini,
-    w_sem,
-    own_sem,
-    out_sem,
-    self_sem,
-    xs_sem,
-    xr_sem,
-    rs_send,
-    relay_sem,
-    fl_sem,
-    fr_sem,
-    ret_send,
-    ret_sem,
-    fin_send,
-    fin_sem,
-):
+HEAD = 128
+ROPE = 64
+PIECE = 512
+UP, DOWN = 4, 3
+
+
+class Attention:
+    def __init__(self, n_z, me, ins, out, buf, sem):
+        self.n_z, self.me, self.ins, self.out, self.buf, self.sem = n_z, me, ins, out, buf, sem
+
+    def prepare(self):
+        me = self.me
+        (queries, kv_latent, rope_key, lat_gain, wk, wv, q_gain, key_gain, rope_gain, _, near, far) = self.ins
+        twice = lambda a: jnp.concatenate([a, a], axis=-1)
+        qn_gain, qr_gain = q_gain[:, :HEAD], twice(q_gain[:, HEAD:])
+        place = me.z * SRC + me.s8
+        far_cos, far_sin = far[0, pl.ds(place, 1)], far[1, pl.ds(place, 1)]
+        cos2 = near[0] * far_cos - near[1] * far_sin
+        sin2 = near[1] * far_cos + near[0] * far_sin
+        kv, rk, kvb, rkb, q_all, qb = (self.buf[k] for k in ("kv", "rk", "kvb", "rkb", "q_all", "qb"))
+        n = queries.shape[0]
+        lane = lax.broadcasted_iota(I32, (n, 128), 1)
+        low = lane < ROPE
+        signed = jnp.where(lane % ROPE < ROPE // 2, -sin2, sin2)
+
+        def turned(v):
+            other = jnp.where(lane % ROPE < ROPE // 2, pltpu.roll(v, 128 - ROPE // 2, 1), pltpu.roll(v, ROPE // 2, 1))
+            return v * cos2 + other * signed
+
+        v = kv_latent[...].astype(F32)
+        latent = (v * lax.rsqrt(jnp.mean(v * v, axis=-1, keepdims=True) + EPS) * lat_gain[...]).astype(BF)
+        keys = dot(latent, wk[...])
+        vals = dot(latent, wv[...]).astype(BF)
+        for h in (0, 1):
+            k = keys[:, HEAD * h : HEAD * (h + 1)]
+            k = k * lax.rsqrt(jnp.mean(k * k, axis=-1, keepdims=True) + EPS) * key_gain[...]
+            kvb[h, :, :HEAD] = k.astype(BF)
+            kvb[h, :, HEAD:] = vals[:, HEAD * h : HEAD * (h + 1)]
+        r = twice(rope_key[...].astype(F32))
+        r = turned(r * lax.rsqrt(jnp.mean(r * r, axis=-1, keepdims=True) + EPS) * twice(rope_gain[...]))
+        rkb[...] = jnp.where(low[: n // 2], r[: n // 2], r[n // 2 :]).astype(BF)
+
+        t0, t1, t2 = (queries[:, 128 * j : 128 * (j + 1)].astype(F32) for j in range(3))
+        total = lambda a: jnp.sum(a, axis=-1, keepdims=True)
+        s1 = t1 * t1
+        width = HEAD + ROPE
+        inv0 = lax.rsqrt((total(t0 * t0) + total(jnp.where(low, s1, 0.0))) / width + EPS)
+        inv1 = lax.rsqrt((total(t2 * t2) + total(jnp.where(low, 0.0, s1))) / width + EPS)
+        nope1 = jnp.where(low, pltpu.roll(t1, ROPE, 1), pltpu.roll(t2, ROPE, 1))
+        turn = turned(jnp.where(low, t1 * inv0, t2 * inv1) * qr_gain)
+        qb[0, :, :HEAD] = (t0 * inv0 * qn_gain).astype(BF)
+        qb[1, :, :HEAD] = (nope1 * inv1 * qn_gain).astype(BF)
+        qb[0, :, HEAD:] = jnp.where(low, turn, 0.0).astype(BF)
+        qb[1, :, HEAD:] = jnp.where(low, 0.0, turn).astype(BF)
+        q_all[me.s8] = qb[me.c]
+        kv[0, self.mine(256)] = kvb[me.c]
+        rk[0, self.mine(128)] = rkb[...]
+
+    def mine(self, n):
+        return pl.ds(pl.multiple_of(self.me.c * n, n), n)
+
+    def send_first(self):
+        me, b, s = self.me, self.buf, self.sem
+        other = (me.z, me.y, 1 - me.c, me.t)
+        remote(b["kvb"].at[1 - me.c], b["kv"].at[0, self.mine(256)], s["kv_out"].at[0], s["kv_in"].at[0], other).start()
+        remote(b["rkb"], b["rk"].at[0, self.mine(128)], s["kv_out"].at[1], s["rk_in"].at[0], other).start()
+
+        def one(i, _):
+            d = (me.s8 + i) % SRC
+            remote(b["qb"].at[d % 2], b["q_all"].at[me.s8], s["q_out"], s["q_in"], me.at(me.z, d)).start()
+            return 0
+
+        lax.fori_loop(1, SRC, one, 0)
+
+    def first_in(self):
+        b, s = self.buf, self.sem
+        await_bytes(b["kvb"].at[0], s["kv_in"].at[0])
+        await_bytes(b["rkb"], s["rk_in"].at[0])
+
+    def queries_in(self):
+        await_bytes(self.buf["q_all"].at[pl.ds(0, SRC - 1)], self.sem["q_in"])
+
+    def has(self, slot):
+        z = self.me.z
+        if slot <= UP:
+            return z >= slot
+        return (z + slot - UP) % self.n_z < DOWN
+
+    def uses(self, slot):
+        z = self.me.z
+        return z >= slot if slot <= UP else z + slot - UP >= self.n_z
+
+    def sends(self, slot, up):
+        z = self.me.z
+        if up:
+            return (z <= self.n_z - 2) & (z >= slot)
+        back = 0 if slot == 0 else slot - UP
+        return (z + back) % self.n_z < DOWN
+
+    def _copies(self, slot, up):
+        me, b, s = self.me, self.buf, self.sem
+        to = slot + 1 if up else (UP + 1 if slot == 0 else slot + 1)
+        z = (me.z + (1 if up else self.n_z - 1)) % self.n_z
+        where = (z, me.y, me.c, me.t)
+        return (
+            remote(b["kv"].at[slot], b["kv"].at[to], s["hop_out"].at[to, 0], s["kv_in"].at[to], where),
+            remote(b["rk"].at[slot], b["rk"].at[to], s["hop_out"].at[to, 1], s["rk_in"].at[to], where),
+        )
+
+    def hop(self, slot, up):
+        @pl.when(self.sends(slot, up))
+        def _():
+            for copy in self._copies(slot, up):
+                copy.start()
+
+    def arrive(self, slot):
+        b, s = self.buf, self.sem
+
+        @pl.when(self.has(slot))
+        def _():
+            await_bytes(b["kv"].at[slot], s["kv_in"].at[slot])
+            await_bytes(b["rk"].at[slot], s["rk_in"].at[slot])
+
+        if slot < UP:
+            self.hop(slot, True)
+        elif UP < slot < UP + DOWN:
+            self.hop(slot, False)
+
+    def attend(self, slot):
+        @pl.when(self.uses(slot))
+        def _():
+            self.load(slot)
+
+            def one(m, _):
+                self.piece(slot, m)
+                return 0
+
+            lax.fori_loop(0, SRC * 256 // PIECE, one, 0)
+
+    def load(self, slot):
+        kv, rk, kop, vop = (self.buf[k] for k in ("kv", "rk", "kop", "vop"))
+        packed = rk[slot].astype(F32)
+        rolled = pltpu.roll(packed, ROPE, 1)
+        low = lax.broadcasted_iota(I32, packed.shape, 1) < ROPE
+        lo = jnp.where(low, packed, rolled).astype(BF)
+        hi = jnp.where(low, rolled, packed).astype(BF)
+        kop[:, :HEAD] = kv[slot, :, :HEAD]
+        for half in (0, 1):
+            kop[256 * half : 256 * half + 128, HEAD:] = lo[128 * half : 128 * half + 128]
+            kop[256 * half + 128 : 256 * half + 256, HEAD:] = hi[128 * half : 128 * half + 128]
+        vop[:, :HEAD] = kv[slot, :, HEAD:]
+
+    def piece(self, slot, m):
+        q_all, acc, kop, vop = (self.buf[k] for k in ("q_all", "acc", "kop", "vop"))
+        n_keys = kop.shape[0]
+        scale = (HEAD + ROPE) ** (-0.5) * math.log2(math.e)
+        two = pl.ds(2 * m, PIECE // 256)
+        q = q_all[two].reshape(PIECE, 2 * HEAD)
+        s = lax.dot_general(q, kop[...], (((1,), (1,)), ((), ())), preferred_element_type=F32)
+        e = jnp.exp2(s * scale)
+        if slot == 0:
+            at_q = lax.broadcasted_iota(I32, (PIECE, n_keys), 0) + m * PIECE
+            at_k = lax.broadcasted_iota(I32, (PIECE, n_keys), 1) + self.me.y * n_keys
+            e = jnp.where(at_q >= at_k, e, 0.0)
+        got = dot(e.astype(BF), vop[...]).reshape(PIECE // 256, 256, 2 * HEAD)
+        if slot == 0:
+            acc[two] = got
+        else:
+            acc[two] += got
+
+    def ones(self):
+        vop = self.buf["vop"]
+        vop[:, HEAD:] = jnp.ones((vop.shape[0], HEAD), BF)
+
+    def send_sums(self):
+        me, b, s = self.me, self.buf, self.sem
+        acc, ob, db, od, dd = (b[k] for k in ("acc", "ob", "db", "od", "dd"))
+
+        def halves(m):
+            a = acc[m]
+            return a[:, :HEAD].astype(BF), jnp.transpose(a[:, HEAD:])[:8]
+
+        def one(i, _):
+            m = (me.s8 + i) % SRC
+            ob[m], db[m] = halves(m)
+            where = me.at(me.z, m)
+            remote(ob.at[m], od.at[me.s8], s["o_out"].at[0], s["o_in"].at[0], where).start()
+            remote(db.at[m], dd.at[me.s8], s["o_out"].at[1], s["o_in"].at[1], where).start()
+            return 0
+
+        lax.fori_loop(1, SRC, one, 0)
+        od[me.s8], dd[me.s8] = halves(me.s8)
+
+    def finish(self):
+        b, s = self.buf, self.sem
+        od, dd = b["od"], b["dd"]
+        out_gain = self.ins[9]
+        await_bytes(od.at[pl.ds(0, SRC - 1)], s["o_in"].at[0])
+        await_bytes(dd.at[pl.ds(0, SRC - 1)], s["o_in"].at[1])
+        for h in (0, 1):
+            o = sum(od[2 * y + h].astype(F32) for y in range(4))
+            d = sum(dd[2 * y + h] for y in range(4))
+            den = jnp.transpose(jnp.broadcast_to(d[0:1], (HEAD, d.shape[1])))
+            m = o / den
+            m = m * lax.rsqrt(jnp.mean(m * m, axis=-1, keepdims=True) + EPS) * out_gain[...]
+            self.out[:, HEAD * h : HEAD * (h + 1)] = m.astype(BF)
+
+    def drain(self):
+        b, s = self.buf, self.sem
+        await_bytes(b["kvb"].at[0], s["kv_out"].at[0])
+        await_bytes(b["rkb"], s["kv_out"].at[1])
+        await_bytes(b["q_all"].at[pl.ds(0, SRC - 1)], s["q_out"])
+        for slot, up in [(k, True) for k in range(UP)] + [(0, False)] + [(UP + k, False) for k in range(1, DOWN)]:
+
+            @pl.when(self.sends(slot, up))
+            def _():
+                for copy in self._copies(slot, up):
+                    copy.wait_send()
+
+        await_bytes(b["od"].at[pl.ds(0, SRC - 1)], s["o_out"].at[0])
+        await_bytes(b["dd"].at[pl.ds(0, SRC - 1)], s["o_out"].at[1])
+
+
+ATT_BUFS = {
+    "kv": ((8, 512, 256), "bf"),
+    "rk": ((8, 256, 128), "bf"),
+    "kvb": ((2, 256, 256), "bf"),
+    "rkb": ((128, 128), "bf"),
+    "q_all": ((8, 256, 256), "bf"),
+    "qb": ((2, 256, 256), "bf"),
+    "acc": ((8, 256, 256), "f"),
+    "kop": ((512, 256), "bf"),
+    "vop": ((512, 256), "bf"),
+    "ob": ((8, 256, 128), "bf"),
+    "db": ((8, 8, 256), "f"),
+    "od": ((8, 256, 128), "bf"),
+    "dd": ((8, 8, 256), "f"),
+}
+ATT_SEMS = {"kv_out": (2,), "kv_in": (8,), "rk_in": (8,), "q_out": None, "q_in": None, "hop_out": (8, 2), "o_out": (2,), "o_in": (2,)}
+
+
+def att_scratch():
+    bufs = [pltpu.VMEM(shape, BF if kind == "bf" else F32) for shape, kind in ATT_BUFS.values()]
+    sems = [pltpu.SemaphoreType.DMA if n is None else pltpu.SemaphoreType.DMA(n) for n in ATT_SEMS.values()]
+    return bufs + sems
+
+
+def att_refs(refs):
+    n = len(ATT_BUFS)
+    return dict(zip(ATT_BUFS, refs[:n])), dict(zip(ATT_SEMS, refs[n:]))
+
+
+OWN = (
+    "wg",
+    "wu",
+    "wd",
+    "normed",
+    "outb",
+    "arr",
+    "rows",
+    "gacc",
+    "uacc",
+    "hid",
+    "wmix",
+    "far",
+    "to_r",
+    "to_l",
+    "relay",
+    "from_l",
+    "from_r",
+    "retb",
+    "reti",
+    "fino",
+    "fini",
+    "w_sem",
+    "own_sem",
+    "out_sem",
+    "xs_sem",
+    "xr_sem",
+    "rs_send",
+    "relay_sem",
+    "fl_sem",
+    "fr_sem",
+    "ret_send",
+    "ret_sem",
+    "fin_send",
+    "fin_sem",
+)
+
+
+def whole_kernel(n_z, *refs):
+    a_in, refs = refs[:12], refs[12:]
+    (tokens, gain, routes_t, weights_t, un_main, un_extra, pk_main, pk_extra, wg_hbm, wu_hbm, wd_hbm), refs = refs[:11], refs[11:]
+    a_out, out, refs = refs[0], refs[1], refs[2:]
+    n_own = len(OWN)
+    own = dict(zip(OWN, refs[:n_own]))
+    wg, wu, wd, normed, outb, arr = (own[k] for k in ("wg", "wu", "wd", "normed", "outb", "arr"))
+    rows, gacc, uacc, hid, wmix, far = (own[k] for k in ("rows", "gacc", "uacc", "hid", "wmix", "far"))
+    to_r, to_l, relay, from_l, from_r, retb = (own[k] for k in ("to_r", "to_l", "relay", "from_l", "from_r", "retb"))
+    reti, fino, fini, w_sem, own_sem, out_sem = (own[k] for k in ("reti", "fino", "fini", "w_sem", "own_sem", "out_sem"))
+    xs_sem, xr_sem, rs_send, relay_sem, fl_sem, fr_sem = (own[k] for k in ("xs_sem", "xr_sem", "rs_send", "relay_sem", "fl_sem", "fr_sem"))
+    ret_send, ret_sem, fin_send, fin_sem = (own[k] for k in ("ret_send", "ret_sem", "fin_send", "fin_sem"))
     me = Place(n_z)
+    att = Attention(n_z, me, a_in, a_out, *att_refs(refs[n_own:]))
     greet(me, n_z)
     loads = [
         pltpu.make_async_copy(h.at[0], v, w_sem.at[k]) for k, (h, v) in enumerate(((wg_hbm, wg), (wu_hbm, wu), (wd_hbm, wd)))
@@ -360,13 +456,18 @@
     lax.fori_loop(0, n_z, dispatch, 0)
     pltpu.make_async_copy(outb.at[0, me.s8], arr.at[0, 0, me.s8], own_sem.at[0]).start()
 
+    att.prepare()
+    att.ones()
+    att.send_first()
+
+    upright = lambda row: jnp.transpose(jnp.broadcast_to(row, (128, n_rows)))[:, 0:1]
     lane_e = lax.broadcasted_iota(I32, (n_rows, 128), 1)
-    ca, cb = routes[:, 0:1], routes[:, 1:2]
+    ca, cb = (upright(r.astype(F32)).astype(I32) for r in (ra, rb))
     on_a, on_b = lane_e == ca, lane_e == cb
     earlier = jnp.where((i1 < i0) & same, 1.0, 0.0).astype(BF)
     count = dot(earlier, jnp.where(on_a | on_b, 1.0, 0.0).astype(BF))
     base = lax.broadcasted_iota(I32, (n_rows, 1), 0) // quarter * 3
-    wa, wb = weights[:, 0:1], weights[:, 1:2]
+    wa, wb = (upright(weights_t[k : k + 1, :]) for k in (0, 1))
 
     def places_c(hit, chosen):
         s = base + jnp.sum(jnp.where(hit, count, 0.0), axis=1, keepdims=True).astype(I32)
@@ -426,8 +527,21 @@
         relay_on(o - 1)
         return 0
 
+    n_pieces = SRC * 256 // PIECE
+
+    def gather_attend(o, _):
+        gather_step(o, 0)
+        att.piece(0, o - (n_z - n_pieces))
+        return 0
+
     gather(0, 0)
-    lax.fori_loop(1, n_z, gather_step, 0)
+    lax.fori_loop(1, n_z - n_pieces, gather_step, 0)
+    att.first_in()
+    att.queries_in()
+    att.load(0)
+    lax.fori_loop(n_z - n_pieces, n_z, gather_attend, 0)
+    att.hop(0, True)
+    att.hop(0, False)
     relay_on(n_z - 1)
 
     loads[0].wait()
@@ -519,10 +633,24 @@
         send_far(first + 2)
         send_side(first + 2, True, False)
         send_side(first, False, False)
+        for slot in (1 + first, 1 + UP + first):
+            att.arrive(slot)
+        for slot in (1 + first, 1 + UP + first):
+            att.attend(slot)
         send_side(first, True, True)
         send_side(first + 2, False, True)
-    for q in (0, 2, 1, 3):
-        finish(q)
+    for slot in (3, 3 + UP):
+        att.arrive(slot)
+    for slot in (3, 3 + UP):
+        att.attend(slot)
+    finish(0)
+    finish(2)
+    att.arrive(4)
+    att.attend(4)
+    att.send_sums()
+    finish(1)
+    finish(3)
+    att.finish()
 
     await_bytes(reti, ret_sem)
     res = reti[...].reshape(64 * MSG, 3 * 128)
@@ -551,24 +679,56 @@
     for buf, sem in ((outb, out_sem), (retb, ret_send)):
         await_bytes(buf.at[pl.ds(1, n_z - 1)], sem)
         await_bytes(buf.at[0, pl.ds(1, SRC - 1)], sem)
-
-
-def experts_part(moe_tokens, moe_gain, routes, route_weights, w_gate, w_up, w_down):
+    att.drain()
+
+
+NEAR = 256
+
+
+def rope_constants(n_places):
+    freqs = 1.0 / THETA ** (np.arange(0, ROPE, 2, dtype=np.float64) / ROPE)
+    freqs = np.tile(freqs.astype(np.float32).astype(np.float64), 4)
+    table = lambda at: jnp.asarray(np.stack([np.cos(at[:, None] * freqs), np.sin(at[:, None] * freqs)]), F32)
+    return table(np.arange(NEAR)), table(np.arange(n_places) * NEAR)
+
+
+def on_device(
+    queries,
+    kv_latent,
+    rope_key,
+    latent_gain,
+    w_key_up,
+    w_value_up,
+    query_gain,
+    key_gain,
+    rope_gain,
+    out_gain,
+    moe_tokens,
+    moe_gain,
+    routes,
+    route_weights,
+    w_gate,
+    w_up,
+    w_down,
+):
     n_z = lax.axis_size("ep_0")
     n_rows, model = moe_tokens.shape
     ff = w_gate.shape[2]
     cols = model // 4
-    consts = fixed_selects()
+    row = lambda g: g.reshape(1, -1)
     vm = pl.BlockSpec(memory_space=pltpu.VMEM)
     hbm = pl.BlockSpec(memory_space=pl.ANY)
     chunk = (4, 192, cols)
     dma = pltpu.SemaphoreType.DMA
     slots = n_z * SRC * CAP
     return pl.pallas_call(
-        functools.partial(experts_kernel, n_z),
-        out_shape=jax.ShapeDtypeStruct((n_rows // 4, model), BF),
-        in_specs=[vm] * 9 + [hbm] * 3,
-        out_specs=vm,
+        functools.partial(whole_kernel, n_z),
+        out_shape=(
+            jax.ShapeDtypeStruct((n_rows, 2 * HEAD), BF),
+            jax.ShapeDtypeStruct((n_rows // 4, model), BF),
+        ),
+        in_specs=[vm] * 20 + [hbm] * 3,
+        out_specs=(vm, vm),
         scratch_shapes=[
             pltpu.VMEM((model, ff), BF),
             pltpu.VMEM((model, ff), BF),
@@ -594,7 +754,6 @@
             dma((3,)),
             dma((n_z,)),
             dma,
-            dma,
             dma((3, 2)),
             dma((3, n_z)),
             dma((3, 4)),
@@ -605,55 +764,31 @@
             dma,
             dma((3,)),
             dma((3,)),
+            *att_scratch(),
         ],
-        compiler_params=pltpu.CompilerParams(collective_id=1, has_side_effects=True, vmem_limit_bytes=60 * 1024 * 1024),
-        name="experts",
+        compiler_params=pltpu.CompilerParams(collective_id=1, has_side_effects=True, vmem_limit_bytes=62 * 1024 * 1024),
+        name="layer",
     )(
+        queries,
+        kv_latent,
+        rope_key,
+        row(latent_gain),
+        w_key_up,
+        w_value_up,
+        row(query_gain),
+        row(key_gain),
+        row(rope_gain),
+        row(out_gain),
+        *rope_constants(n_z * SRC),
         moe_tokens,
-        moe_gain.reshape(1, model),
-        routes,
+        row(moe_gain),
         routes.T,
-        route_weights,
-        *consts,
+        route_weights.T,
+        *fixed_selects(),
         w_gate,
         w_up,
         w_down,
     )
-
-
-def on_device(
-    queries,
-    kv_latent,
-    rope_key,
-    latent_gain,
-    w_key_up,
-    w_value_up,
-    query_gain,
-    key_gain,
-    rope_gain,
-    out_gain,
-    moe_tokens,
-    moe_gain,
-    routes,
-    route_weights,
-    w_gate,
-    w_up,
-    w_down,
-):
-    attended = attention_part(
-        queries,
-        kv_latent,
-        rope_key,
-        latent_gain,
-        w_key_up,
-        w_value_up,
-        query_gain,
-        key_gain,
-        rope_gain,
-        out_gain,
-    )
-    moe_out = experts_part(moe_tokens, moe_gain, routes, route_weights, w_gate, w_up, w_down)
-    return (attended, moe_out)
 
 
 def solution(mesh):

time: 310 us -> 128 us (0.41)
  the two profiles are of different devices: /device:TPU:251 before, /device:TPU:1 now
where the time goes in v3:
time: 128 us; the launch traced here: 127 us
  Pallas kernels  122 us (95%)
  local copies, waits for them, and re-layouts  4.73 us (4%)
    pallas_call x1, Pallas kernels, on_device(): pl.pallas_call(functools.partial(whole_kernel, n_z), out_shape=(jax.Shape...  122 us
    unnamed x3, local copies, waits for them, and re-layouts  4.73 us

profile of v3, /device:TPU:1, one launch (start us, length us, event | category | flops | bytes accessed | tf_op | source)
XLA Modules:
  0.0 127.4 jit_solution(12142941247037713502)
XLA Ops:
  0.6 1.5 %copy.25.refs_2_ = bf16[256,64]{1,0:T(8,128)(2,1)} copy(bf16[256,64]{0,1:T(8,128)(2,1)} %param.25) | data formatting | bytes 65536 | tf_op args[2]
  2.1 122.1 %layer.1 = (bf16[256,256]{1,0:T(8,128)(2,1)}, bf16[64,2048]{1,0:T(8,128)(2,1)}) custom-call(bf16[256,384]{1,0:T(8,128)(2,1)} %refs_0_.1, bf16[256,512]{1,0:T(8,128)(2,1)} %refs_1_.1, bf16[256,64]{1,0:T(8,128)(2,1)} %copy.25.refs_2_, f32[1,512]{1,0:T(1,128)} %bitcast.9, bf16[512,256]{1,0:T(8,128)(2,1)} %refs_4_.1, bf16[512,256]{1,0:T(8,128)(2,1)} %refs_5_.1, ...), custom_call_target="tpu_custom_call" | custom-call | tf_op jit(solution)/shard_map/layer/pallas_call | solution.py:724
  124.2 1.6 %copy.28 = bf16[256,256]{1,0:T(8,128)(2,1)} copy(bf16[256,256]{1,0:T(8,128)(2,1)} %get-tuple-element.4) | data formatting | bytes 262144
  125.8 1.7 %copy.29 = bf16[64,2048]{1,0:T(8,128)(2,1)} copy(bf16[64,2048]{1,0:T(8,128)(2,1)} %get-tuple-element.5) | data formatting | bytes 524288

commit v4 on v3

--- a/solution.py
+++ b/solution.py
@@ -12,6 +12,7 @@
 
 BF, F32, I32 = jnp.bfloat16, jnp.float32, jnp.int32
 MESH = pl.DeviceIdType.MESH
+Z_ORDER = (0, 1, 7, 4, 3, 5, 2, 6)
 
 EP = ("ep_0", "ep_1", "ep_2")
 EP_TP = ("ep_0", "ep_1", "ep_2", "tp")
@@ -52,8 +53,7 @@
         self.s8 = self.y * 2 + self.c
 
     def row(self, order):
-        up = order % 2
-        return up * ((order + 1) // 2) + (1 - up) * ((self.n_z - order // 2) % self.n_z)
+        return sum(jnp.where(order == k, d, 0) for k, d in enumerate(Z_ORDER))
 
     def x(self, step):
         return (self.z, self.y, self.c, (self.t + step) % 4)
@@ -96,7 +96,8 @@
 HEAD = 128
 ROPE = 64
 PIECE = 512
-UP, DOWN = 4, 3
+HOP_AT, QUERY_AT, FIRST_AT, PAIR_AT, SUMS_AT = 1, 1, 2, 2, 6
+UP, DOWN = 3, 4
 
 
 class Attention:
@@ -131,7 +132,8 @@
             k = k * lax.rsqrt(jnp.mean(k * k, axis=-1, keepdims=True) + EPS) * key_gain[...]
             kvb[h, :, :HEAD] = k.astype(BF)
             kvb[h, :, HEAD:] = vals[:, HEAD * h : HEAD * (h + 1)]
-        r = twice(rope_key[...].astype(F32))
+        flat = rope_key[...].astype(F32)
+        r = jnp.transpose(jnp.concatenate([flat, flat], axis=0))
         r = turned(r * lax.rsqrt(jnp.mean(r * r, axis=-1, keepdims=True) + EPS) * twice(rope_gain[...]))
         rkb[...] = jnp.where(low[: n // 2], r[: n // 2], r[n // 2 :]).astype(BF)
 
@@ -160,6 +162,9 @@
         remote(b["kvb"].at[1 - me.c], b["kv"].at[0, self.mine(256)], s["kv_out"].at[0], s["kv_in"].at[0], other).start()
         remote(b["rkb"], b["rk"].at[0, self.mine(128)], s["kv_out"].at[1], s["rk_in"].at[0], other).start()
 
+    def send_queries(self):
+        me, b, s = self.me, self.buf, self.sem
+
         def one(i, _):
             d = (me.s8 + i) % SRC
             remote(b["qb"].at[d % 2], b["q_all"].at[me.s8], s["q_out"], s["q_in"], me.at(me.z, d)).start()
@@ -177,24 +182,22 @@
 
     def has(self, slot):
         z = self.me.z
-        if slot <= UP:
-            return z >= slot
-        return (z + slot - UP) % self.n_z < DOWN
+        return jnp.where(slot <= UP, z >= slot, (z + slot - UP) % self.n_z < DOWN)
 
     def uses(self, slot):
         z = self.me.z
-        return z >= slot if slot <= UP else z + slot - UP >= self.n_z
+        return jnp.where(slot <= UP, z >= slot, z + slot - UP >= self.n_z)
 
     def sends(self, slot, up):
         z = self.me.z
         if up:
-            return (z <= self.n_z - 2) & (z >= slot)
-        back = 0 if slot == 0 else slot - UP
-        return (z + back) % self.n_z < DOWN
+            return (z <= self.n_z - 2) & (z >= slot) & (slot < UP)
+        back = jnp.where(slot == 0, 0, slot - UP)
+        return ((z + back) % self.n_z < DOWN) & ((slot == 0) | ((slot > UP) & (slot < UP + DOWN)))
 
     def _copies(self, slot, up):
         me, b, s = self.me, self.buf, self.sem
-        to = slot + 1 if up else (UP + 1 if slot == 0 else slot + 1)
+        to = slot + 1 if up else jnp.where(slot == 0, UP + 1, slot + 1)
         z = (me.z + (1 if up else self.n_z - 1)) % self.n_z
         where = (z, me.y, me.c, me.t)
         return (
@@ -216,21 +219,59 @@
             await_bytes(b["kv"].at[slot], s["kv_in"].at[slot])
             await_bytes(b["rk"].at[slot], s["rk_in"].at[slot])
 
-        if slot < UP:
-            self.hop(slot, True)
-        elif UP < slot < UP + DOWN:
-            self.hop(slot, False)
-
-    def attend(self, slot):
-        @pl.when(self.uses(slot))
-        def _():
-            self.load(slot)
-
-            def one(m, _):
-                self.piece(slot, m)
-                return 0
-
-            lax.fori_loop(0, SRC * 256 // PIECE, one, 0)
+        self.hop(slot, True)
+        self.hop(slot, False)
+
+    def pairs(self, j, done):
+        def arrive(side, _):
+            slot = j + side * UP
+
+            @pl.when((slot < 8) & ((side == 1) | (slot <= UP)))
+            def _():
+                self.arrive(slot)
+
+            return 0
+
+        def attend(side, _):
+            slot = j + side * UP
+
+            @pl.when((slot < 8) & ((side == 1) | (slot <= UP)) & self.uses(slot))
+            def _():
+                self.attend(slot, False)
+
+            return 0
+
+        lax.fori_loop(0, 2, attend if done else arrive, 0)
+
+    def attend(self, slot, diagonal):
+        self.load(slot)
+        q_all, acc, kop, vop = (self.buf[k] for k in ("q_all", "acc", "kop", "vop"))
+        n_keys = kop.shape[0]
+        scale = (HEAD + ROPE) ** (-0.5) * math.log2(math.e)
+        keys, vals = kop[...], vop[...]
+        count, per = SRC * 256 // PIECE, PIECE // 256
+
+        def score(m):
+            q = q_all[per * m : per * (m + 1)].reshape(PIECE, 2 * HEAD)
+            return lax.dot_general(q, keys, (((1,), (1,)), ((), ())), preferred_element_type=F32)
+
+        def weigh(m, s):
+            e = jnp.exp2(s * scale)
+            if diagonal:
+                at_q = lax.broadcasted_iota(I32, (PIECE, n_keys), 0) + m * PIECE
+                at_k = lax.broadcasted_iota(I32, (PIECE, n_keys), 1) + self.me.y * n_keys
+                e = jnp.where(at_q >= at_k, e, 0.0)
+            got = dot(e.astype(BF), vals).reshape(per, 256, 2 * HEAD)
+            if diagonal:
+                acc[per * m : per * (m + 1)] = got
+            else:
+                acc[per * m : per * (m + 1)] += got
+
+        s = score(0)
+        for m in range(count):
+            ahead = score(m + 1) if m + 1 < count else None
+            weigh(m, s)
+            s = ahead
 
     def load(self, slot):
         kv, rk, kop, vop = (self.buf[k] for k in ("kv", "rk", "kop", "vop"))
@@ -244,24 +285,6 @@
             kop[256 * half : 256 * half + 128, HEAD:] = lo[128 * half : 128 * half + 128]
             kop[256 * half + 128 : 256 * half + 256, HEAD:] = hi[128 * half : 128 * half + 128]
         vop[:, :HEAD] = kv[slot, :, HEAD:]
-
-    def piece(self, slot, m):
-        q_all, acc, kop, vop = (self.buf[k] for k in ("q_all", "acc", "kop", "vop"))
-        n_keys = kop.shape[0]
-        scale = (HEAD + ROPE) ** (-0.5) * math.log2(math.e)
-        two = pl.ds(2 * m, PIECE // 256)
-        q = q_all[two].reshape(PIECE, 2 * HEAD)
-        s = lax.dot_general(q, kop[...], (((1,), (1,)), ((), ())), preferred_element_type=F32)
-        e = jnp.exp2(s * scale)
-        if slot == 0:
-            at_q = lax.broadcasted_iota(I32, (PIECE, n_keys), 0) + m * PIECE
-            at_k = lax.broadcasted_iota(I32, (PIECE, n_keys), 1) + self.me.y * n_keys
-            e = jnp.where(at_q >= at_k, e, 0.0)
-        got = dot(e.astype(BF), vop[...]).reshape(PIECE // 256, 256, 2 * HEAD)
-        if slot == 0:
-            acc[two] = got
-        else:
-            acc[two] += got
 
     def ones(self):
         vop = self.buf["vop"]
@@ -345,16 +368,14 @@
     return dict(zip(ATT_BUFS, refs[:n])), dict(zip(ATT_SEMS, refs[n:]))
 
 
+BIG = ("tokens", "queries", "kv_latent", "w_key", "w_val", "near", "un_main", "un_extra", "pk_main", "pk_extra")
 OWN = (
-    "wg",
-    "wu",
+    "wgu",
     "wd",
     "normed",
     "outb",
     "arr",
     "rows",
-    "gacc",
-    "uacc",
     "hid",
     "wmix",
     "far",
@@ -384,22 +405,32 @@
 
 
 def whole_kernel(n_z, *refs):
-    a_in, refs = refs[:12], refs[12:]
-    (tokens, gain, routes_t, weights_t, un_main, un_extra, pk_main, pk_extra, wg_hbm, wu_hbm, wd_hbm), refs = refs[:11], refs[11:]
+    n_small, n_big, n_own = 10, len(BIG), len(OWN)
+    (lat_gain, q_gain, key_gain, rope_gain, out_gain, far_table, rope_key, gain, routes_t, weights_t) = refs[:n_small]
+    refs = refs[n_small:]
+    big_hbm, (wg_hbm, wu_hbm, wd_hbm), refs = refs[:n_big], refs[n_big : n_big + 3], refs[n_big + 3 :]
     a_out, out, refs = refs[0], refs[1], refs[2:]
-    n_own = len(OWN)
     own = dict(zip(OWN, refs[:n_own]))
-    wg, wu, wd, normed, outb, arr = (own[k] for k in ("wg", "wu", "wd", "normed", "outb", "arr"))
-    rows, gacc, uacc, hid, wmix, far = (own[k] for k in ("rows", "gacc", "uacc", "hid", "wmix", "far"))
-    to_r, to_l, relay, from_l, from_r, retb = (own[k] for k in ("to_r", "to_l", "relay", "from_l", "from_r", "retb"))
-    reti, fino, fini, w_sem, own_sem, out_sem = (own[k] for k in ("reti", "fino", "fini", "w_sem", "own_sem", "out_sem"))
-    xs_sem, xr_sem, rs_send, relay_sem, fl_sem, fr_sem = (own[k] for k in ("xs_sem", "xr_sem", "rs_send", "relay_sem", "fl_sem", "fr_sem"))
-    ret_send, ret_sem, fin_send, fin_sem = (own[k] for k in ("ret_send", "ret_sem", "fin_send", "fin_sem"))
+    big, big_sem, refs = refs[n_own : n_own + n_big], refs[n_own + n_big], refs[n_own + n_big + 1 :]
+    (tokens, queries, kv_latent, w_key, w_val, near_table, un_main, un_extra, pk_main, pk_extra) = big
+    takes = [pltpu.make_async_copy(h, v, big_sem.at[k]) for k, (h, v) in enumerate(zip(big_hbm, big))]
+    for take in takes:
+        take.start()
+    a_in = (queries, kv_latent, rope_key, lat_gain, w_key, w_val, q_gain, key_gain, rope_gain, out_gain, near_table, far_table)
+    wgu, wd, normed, outb, arr, rows = (own[k] for k in ("wgu", "wd", "normed", "outb", "arr", "rows"))
+    hid, wmix, far, to_r, to_l, relay = (own[k] for k in ("hid", "wmix", "far", "to_r", "to_l", "relay"))
+    from_l, from_r, retb, reti, fino, fini = (own[k] for k in ("from_l", "from_r", "retb", "reti", "fino", "fini"))
+    w_sem, own_sem, out_sem, xs_sem, xr_sem, rs_send = (own[k] for k in ("w_sem", "own_sem", "out_sem", "xs_sem", "xr_sem", "rs_send"))
+    relay_sem, fl_sem, fr_sem, ret_send, ret_sem, fin_send = (own[k] for k in ("relay_sem", "fl_sem", "fr_sem", "ret_send", "ret_sem", "fin_send"))
+    fin_sem = own["fin_sem"]
     me = Place(n_z)
-    att = Attention(n_z, me, a_in, a_out, *att_refs(refs[n_own:]))
+    att = Attention(n_z, me, a_in, a_out, *att_refs(refs))
     greet(me, n_z)
+    ff = wd.shape[0]
     loads = [
-        pltpu.make_async_copy(h.at[0], v, w_sem.at[k]) for k, (h, v) in enumerate(((wg_hbm, wg), (wu_hbm, wu), (wd_hbm, wd)))
+        pltpu.make_async_copy(wg_hbm.at[0], wgu.at[:, pl.ds(0, ff)], w_sem.at[0]),
+        pltpu.make_async_copy(wu_hbm.at[0], wgu.at[:, pl.ds(ff, ff)], w_sem.at[1]),
+        pltpu.make_async_copy(wd_hbm.at[0], wd, w_sem.at[2]),
     ]
     for load in loads:
         load.start()
@@ -424,6 +455,7 @@
 
     (ma, xa), (mb, xb) = places(hit_a, ra), places(hit_b, rb)
 
+    takes[0].wait()
     v = tokens[...].astype(F32)
     scale = lax.rsqrt(jnp.mean(v * v, axis=-1, keepdims=True) + EPS)
     mine = pl.ds(pl.multiple_of(me.t * cols, cols), cols)
@@ -456,10 +488,6 @@
     lax.fori_loop(0, n_z, dispatch, 0)
     pltpu.make_async_copy(outb.at[0, me.s8], arr.at[0, 0, me.s8], own_sem.at[0]).start()
 
-    att.prepare()
-    att.ones()
-    att.send_first()
-
     upright = lambda row: jnp.transpose(jnp.broadcast_to(row, (128, n_rows)))[:, 0:1]
     lane_e = lax.broadcasted_iota(I32, (n_rows, 128), 1)
     ca, cb = (upright(r.astype(F32)).astype(I32) for r in (ra, rb))
@@ -485,29 +513,28 @@
         wmix[k, 1] = lo
         return 0
 
-    lax.fori_loop(0, 4, mix, 0)
 
     def pass_on(b, o, step, dst):
         remote(arr.at[b, o], arr.at[dst, o], xs_sem.at[b, step % 4 // 2], xr_sem.at[dst - 1, o], me.x(step)).start()
 
-    def unpack(b, p):
+    def rank_cols(rank, width=cols, skip=0):
+        return pl.ds(pl.multiple_of((me.t + rank) % 4 * cols + skip, 128), width)
+
+    def unpack(b, rank, p):
         packed = arr[b, pl.ds(2 * p, 2)].reshape(2 * SRC * MSG, 3 * 128)
         tiles = jnp.concatenate([packed[:, 128 * j : 128 * (j + 1)] for j in range(3)], axis=0)
-        r = pl.ds(pl.multiple_of(p * 192, 192), 192)
-        rows[b, r, : 3 * 128] = dot(un_main[...], packed).astype(BF)
-        rows[b, r, 3 * 128 :] = dot(un_extra[...], tiles).astype(BF)
-
-    def gather(o, _):
+        rows[:, rank_cols(rank, 3 * 128)] = dot(un_main[...], packed).astype(BF)
+        rows[:, rank_cols(rank, 128, 3 * 128)] = dot(un_extra[...], tiles).astype(BF)
+
+    def unpack_near(p):
+        for b, rank in ((0, 0), (1, 3), (2, 1)):
+            unpack(b, rank, p)
+
+    def gather(o):
         await_bytes(arr.at[0, o], own_sem.at[o])
         pass_on(0, o, 1, 1)
         pass_on(0, o, 3, 2)
 
-        @pl.when(o % 2 == 1)
-        def _():
-            unpack(0, o // 2)
-
-        return 0
-
     def relay_on(o):
         await_bytes(arr.at[1, o], xr_sem.at[0, o])
         await_bytes(arr.at[2, o], xr_sem.at[1, o])
@@ -519,93 +546,34 @@
         @pl.when(o % 2 == 1)
         def _():
             pass_on(2, o, 3, 3)
-            unpack(1, o // 2)
-            unpack(2, o // 2)
-
-    def gather_step(o, _):
-        gather(o, 0)
-        relay_on(o - 1)
-        return 0
-
-    n_pieces = SRC * 256 // PIECE
-
-    def gather_attend(o, _):
-        gather_step(o, 0)
-        att.piece(0, o - (n_z - n_pieces))
-        return 0
-
-    gather(0, 0)
-    lax.fori_loop(1, n_z - n_pieces, gather_step, 0)
-    att.first_in()
-    att.queries_in()
-    att.load(0)
-    lax.fori_loop(n_z - n_pieces, n_z, gather_attend, 0)
-    att.hop(0, True)
-    att.hop(0, False)
-    relay_on(n_z - 1)
-
-    loads[0].wait()
-    loads[1].wait()
-    n_all = rows.shape[1]
-    part = 192
-    sides = ((0, 0), (1, 3), (2, 1), (3, 2))
-
-    def up_gate(b, rank, first):
-        k = pl.ds(pl.multiple_of((me.t + rank) % 4 * cols, cols), cols)
-
-        def one(m, _):
-            r = pl.ds(pl.multiple_of(m * part, part), part)
-            lhs = rows[b, r]
-            g, u = dot(lhs, wg[k, :]), dot(lhs, wu[k, :])
-            if first:
-                gacc[r] = g
-                uacc[r] = u
-            else:
-                gacc[r] += g
-                uacc[r] += u
-            return 0
-
-        lax.fori_loop(0, n_all // part, one, 0)
-
-    up_gate(0, 0, True)
-    up_gate(1, 3, False)
-    up_gate(2, 1, False)
-
-    def last_pair(p, _):
+
+    def down(q, rank):
+        return dot(hid[q], wd[:, rank_cols(rank)])
+
+    half = 96
+    parts = (pl.ds(0, half), pl.ds(half, half))
+
+    def hidden_units(p):
         await_bytes(arr.at[3, 2 * p], xr_sem.at[2, 2 * p])
         await_bytes(arr.at[3, 2 * p + 1], xr_sem.at[2, 2 * p + 1])
-        unpack(3, p)
-        return 0
-
-    lax.fori_loop(0, n_z // 2, last_pair, 0)
-    k3 = pl.ds(pl.multiple_of((me.t + 2) % 4 * cols, cols), cols)
-
-    def act(m, _):
-        r = pl.ds(pl.multiple_of(m * part, part), part)
-        lhs = rows[3, r]
-        g = gacc[r] + dot(lhs, wg[k3, :])
-        u = uacc[r] + dot(lhs, wu[k3, :])
-        hid[r] = (g / (1.0 + jnp.exp(-g)) * u).astype(BF)
-        return 0
-
-    lax.fori_loop(0, n_all // part, act, 0)
-    loads[2].wait()
-
-    def down(q, rank):
-        return dot(hid[q * part : (q + 1) * part], wd[:, pl.ds(pl.multiple_of((me.t + rank) % 4 * cols, cols), cols)])
-
-    def send_far(q):
-        far[q] = down(q, 2).astype(BF)
-        remote(far.at[q], relay.at[q], rs_send.at[0, q], relay_sem.at[q], me.x(1 if q < 2 else 3)).start()
-
-    def send_side(q, right, add):
-        buf, dst, sem, rank = (to_r, from_l, fl_sem, 1) if right else (to_l, from_r, fr_sem, 3)
-        y = down(q, rank)
-        if add:
-            await_bytes(relay.at[q], relay_sem.at[q])
-            y = y + relay[q].astype(F32)
-        buf[q] = y.astype(BF)
-        remote(buf.at[q], dst.at[q], rs_send.at[1 if right else 2, q], sem.at[q], me.x(1 if right else 3)).start()
+        unpack(3, 2, p)
+        gu = dot(rows[...], wgu[...])
+        g, u = gu[:, :ff], gu[:, ff:]
+        hid[p] = (g / (1.0 + jnp.exp(-g)) * u).astype(BF)
+        far[p] = down(p, 2).astype(BF)
+        for k, step in ((0, 1), (1, 3)):
+            remote(far.at[p, parts[k]], relay.at[p, parts[k]], rs_send.at[0, p, k], relay_sem.at[p, k], me.x(step)).start()
+
+    def sides(q):
+        await_bytes(relay.at[q, parts[0]], relay_sem.at[q, 0])
+        await_bytes(relay.at[q, parts[1]], relay_sem.at[q, 1])
+        for k, (buf, dst, sem, rank) in enumerate(((to_r, from_l, fl_sem, 1), (to_l, from_r, fr_sem, 3))):
+            y = down(q, rank)
+            added = y[half * k : half * (k + 1)] + relay[q, parts[k]].astype(F32)
+            kept = y[half * (1 - k) : half * (2 - k)]
+            buf[q, parts[k]] = added.astype(BF)
+            buf[q, parts[1 - k]] = kept.astype(BF)
+            remote(buf.at[q], dst.at[q], rs_send.at[1 + k, q, 0], sem.at[q], me.x(rank)).start()
 
     def finish(q):
         y = down(q, 0)
@@ -614,42 +582,99 @@
         y = (y + from_l[q].astype(F32) + from_r[q].astype(F32)).astype(BF)
         ext = dot(pk_extra[...], y[:, 3 * 128 :])
         packed = dot(pk_main[...], y[:, : 3 * 128]) + jnp.concatenate([ext[256 * j : 256 * (j + 1)] for j in range(3)], axis=1)
-        retb[2 * q : 2 * q + 2] = packed.astype(BF).reshape(2, SRC, MSG, 3 * 128)
+        retb[pl.ds(2 * q, 2)] = packed.astype(BF).reshape(2, SRC, MSG, 3 * 128)
         mine_e = me.z * SRC + me.s8
-        for o in (2 * q, 2 * q + 1):
+
+        def send(i, _):
+            o = 2 * q + i // SRC
             z = (me.z - me.row(o) + n_z) % n_z
-
-            def send(i, _):
-                s = (me.s8 + i) % SRC
-                remote(retb.at[o, s], reti.at[mine_e], ret_send, ret_sem, me.at(z, s)).start()
-                return 0
-
-            lax.fori_loop(1 if o == 0 else 0, SRC, send, 0)
-        if q == 0:
+            s = (me.s8 + i) % SRC
+            remote(retb.at[o, s], reti.at[mine_e], ret_send, ret_sem, me.at(z, s)).start()
+            return 0
+
+        lax.fori_loop(jnp.where(q == 0, 1, 0), 2 * SRC, send, 0)
+
+        @pl.when(q == 0)
+        def _():
             pltpu.make_async_copy(retb.at[0, me.s8], reti.at[mine_e], ret_sem).start()
 
-    for first in (0, 1):
-        send_far(first)
-        send_far(first + 2)
-        send_side(first + 2, True, False)
-        send_side(first, False, False)
-        for slot in (1 + first, 1 + UP + first):
-            att.arrive(slot)
-        for slot in (1 + first, 1 + UP + first):
-            att.attend(slot)
-        send_side(first, True, True)
-        send_side(first + 2, False, True)
-    for slot in (3, 3 + UP):
-        att.arrive(slot)
-    for slot in (3, 3 + UP):
-        att.attend(slot)
-    finish(0)
-    finish(2)
-    att.arrive(4)
-    att.attend(4)
-    att.send_sums()
-    finish(1)
-    finish(3)
+    n_pairs = n_z // 2
+
+    def step(k, _):
+        @pl.when(k < n_pairs)
+        def _():
+            gather(2 * k)
+
+            @pl.when(k == 0)
+            def _():
+                for take in takes[1:]:
+                    take.wait()
+                att.prepare()
+                att.ones()
+                att.send_first()
+                lax.fori_loop(0, 4, mix, 0)
+
+            @pl.when(k > 0)
+            def _():
+                relay_on(2 * k - 1)
+                unpack_near(k - 1)
+
+            gather(2 * k + 1)
+            relay_on(2 * k)
+
+        @pl.when(k == n_pairs)
+        def _():
+            relay_on(n_z - 1)
+            unpack_near(n_pairs - 1)
+
+        @pl.when(k == QUERY_AT)
+        def _():
+            att.send_queries()
+
+        @pl.when(k == HOP_AT)
+        def _():
+            att.first_in()
+            att.hop(0, True)
+            att.hop(0, False)
+
+        @pl.when((k >= PAIR_AT) & (k < PAIR_AT + DOWN))
+        def _():
+            att.pairs(k - PAIR_AT + 1, False)
+
+        @pl.when((k >= 3) & (k < n_pairs + 3))
+        def _():
+            finish(k - 3)
+
+        @pl.when((k >= 2) & (k < n_pairs + 2))
+        def _():
+            sides(k - 2)
+
+        @pl.when((k >= 1) & (k < n_pairs + 1))
+        def _():
+            @pl.when(k == 1)
+            def _():
+                loads[0].wait()
+                loads[1].wait()
+                loads[2].wait()
+
+            hidden_units(k - 1)
+
+        @pl.when(k == FIRST_AT)
+        def _():
+            att.queries_in()
+            att.attend(0, True)
+
+        @pl.when((k >= PAIR_AT) & (k < PAIR_AT + DOWN))
+        def _():
+            att.pairs(k - PAIR_AT + 1, True)
+
+        @pl.when(k == jnp.where(me.z > DOWN - 1, SUMS_AT, jnp.where(me.z == 0, FIRST_AT, PAIR_AT + me.z - 1)))
+        def _():
+            att.send_sums()
+
+        return 0
+
+    lax.fori_loop(0, n_pairs + 3, step, 0)
     att.finish()
 
     await_bytes(reti, ret_sem)
@@ -672,8 +697,9 @@
     for step in (0, 1, 2):
         await_bytes(fini.at[step], fin_send.at[step])
     for q in range(4):
-        for k in range(3):
-            await_bytes(far.at[q], rs_send.at[k, q])
+        for k in (0, 1):
+            await_bytes(far.at[q, parts[k]], rs_send.at[0, q, k])
+            await_bytes(far.at[q], rs_send.at[1 + k, q, 0])
     for b, k, n in ((0, 0, n_z), (0, 1, n_z), (1, 0, n_z // 2), (2, 1, n_z // 2)):
         await_bytes(arr.at[b, pl.ds(0, n)], xs_sem.at[b, k])
     for buf, sem in ((outb, out_sem), (retb, ret_send)):
@@ -719,34 +745,29 @@
     vm = pl.BlockSpec(memory_space=pltpu.VMEM)
     hbm = pl.BlockSpec(memory_space=pl.ANY)
     chunk = (4, 192, cols)
+    near, far = rope_constants(n_z * SRC)
+    small = tuple(row(g) for g in (latent_gain, query_gain, key_gain, rope_gain, out_gain))
+    small += (far, rope_key.T, row(moe_gain), routes.T, route_weights.T)
+    big = (moe_tokens, queries, kv_latent, w_key_up, w_value_up, near, *fixed_selects())
     dma = pltpu.SemaphoreType.DMA
-    slots = n_z * SRC * CAP
     return pl.pallas_call(
         functools.partial(whole_kernel, n_z),
         out_shape=(
             jax.ShapeDtypeStruct((n_rows, 2 * HEAD), BF),
             jax.ShapeDtypeStruct((n_rows // 4, model), BF),
         ),
-        in_specs=[vm] * 20 + [hbm] * 3,
+        in_specs=[vm] * len(small) + [hbm] * (len(big) + 3),
         out_specs=(vm, vm),
         scratch_shapes=[
-            pltpu.VMEM((model, ff), BF),
-            pltpu.VMEM((model, ff), BF),
+            pltpu.VMEM((model, 2 * ff), BF),
             pltpu.VMEM((ff, model), BF),
             pltpu.VMEM((n_rows, cols), BF),
             pltpu.VMEM((n_z, SRC, MSG, 384), BF),
             pltpu.VMEM((4, n_z, SRC, MSG, 384), BF),
-            pltpu.VMEM((4, slots, cols), BF),
-            pltpu.VMEM((slots, ff), F32),
-            pltpu.VMEM((slots, ff), F32),
-            pltpu.VMEM((slots, ff), BF),
+            pltpu.VMEM((192, model), BF),
+            pltpu.VMEM((4, 192, ff), BF),
             pltpu.VMEM((4, 2, n_rows, 64 * MSG), BF),
-            pltpu.VMEM(chunk, BF),
-            pltpu.VMEM(chunk, BF),
-            pltpu.VMEM(chunk, BF),
-            pltpu.VMEM(chunk, BF),
-            pltpu.VMEM(chunk, BF),
-            pltpu.VMEM(chunk, BF),
+            *[pltpu.VMEM(chunk, BF)] * 6,
             pltpu.VMEM((n_z, SRC, MSG, 384), BF),
             pltpu.VMEM((n_z * SRC, MSG, 384), BF),
             pltpu.VMEM((4, n_rows // 4, cols), BF),
@@ -756,35 +777,23 @@
             dma,
             dma((3, 2)),
             dma((3, n_z)),
-            dma((3, 4)),
-            dma((4,)),
+            dma((3, 4, 2)),
+            dma((4, 2)),
             dma((4,)),
             dma((4,)),
             dma,
             dma,
             dma((3,)),
             dma((3,)),
+            *[pltpu.VMEM(a.shape, a.dtype) for a in big],
+            dma((len(big),)),
             *att_scratch(),
         ],
         compiler_params=pltpu.CompilerParams(collective_id=1, has_side_effects=True, vmem_limit_bytes=62 * 1024 * 1024),
         name="layer",
     )(
-        queries,
-        kv_latent,
-        rope_key,
-        row(latent_gain),
-        w_key_up,
-        w_value_up,
-        row(query_gain),
-        row(key_gain),
-        row(rope_gain),
-        row(out_gain),
-        *rope_constants(n_z * SRC),
-        moe_tokens,
-        row(moe_gain),
-        routes.T,
-        route_weights.T,
-        *fixed_selects(),
+        *small,
+        *big,
         w_gate,
         w_up,
         w_down,

time: 128 us -> 106 us (0.83)
  Pallas kernels: 122 us -> 102 us
  local copies, waits for them, and re-layouts: 4.73 us -> 3.24 us
    pallas_call x1, Pallas kernels: 122 us -> 102 us  [on_device(): pl.pallas_call(functools.partial(whole_kernel, n_z), out_shape=(jax.Shape...]
    unnamed x3 -> x2, local copies, waits for them, and re-layouts: 4.73 us -> 3.24 us
where the time goes in v4:
time: 106 us
  Pallas kernels  102 us (96%)
  local copies, waits for them, and re-layouts  3.24 us (3%)
    pallas_call x1, Pallas kernels, on_device(): pl.pallas_call(functools.partial(whole_kernel, n_z), out_shape=(jax.Shape...  102 us
    unnamed x2, local copies, waits for them, and re-layouts  3.24 us

profile of v4, /device:TPU:1, one launch (start us, length us, event | category | flops | bytes accessed | tf_op | source)
XLA Modules:
  0.0 105.6 jit_solution(5460984156235684529)
XLA Ops:
  0.6 101.7 %layer.1 = (bf16[256,256]{1,0:T(8,128)(2,1)}, bf16[64,2048]{1,0:T(8,128)(2,1)}) custom-call(f32[1,512]{1,0:T(1,128)} %bitcast.11, f32[1,192]{1,0:T(1,128)} %bitcast.14, f32[1,128]{1,0:T(1,128)} %bitcast.15, f32[1,64]{1,0:T(1,128)} %bitcast.16, f32[1,128]{1,0:T(1,128)} %bitcast.17, f32[2,64,128]{2,1,0:T(8,128)} %constant.13.clone.refs_5_, ...), custom_call_target="tpu_custom_call" | custom-call | tf_op jit(solution)/shard_map/layer/pallas_call | solution.py:753
  102.4 1.6 %copy.27 = bf16[256,256]{1,0:T(8,128)(2,1)} copy(bf16[256,256]{1,0:T(8,128)(2,1)} %get-tuple-element.4) | data formatting | bytes 262144
  104.0 1.7 %copy.28 = bf16[64,2048]{1,0:T(8,128)(2,1)} copy(bf16[64,2048]{1,0:T(8,128)(2,1)} %get-tuple-element.5) | data formatting | bytes 524288

commit v5 on v4

--- a/solution.py
+++ b/solution.py
@@ -96,7 +96,7 @@
 HEAD = 128
 ROPE = 64
 PIECE = 512
-HOP_AT, QUERY_AT, FIRST_AT, PAIR_AT, SUMS_AT = 1, 1, 2, 2, 6
+HOP_AT, QUERY_AT, FIRST_AT, PAIR_AT = 1, 1, 2, 2
 UP, DOWN = 3, 4
 
 
@@ -290,34 +290,65 @@
         vop = self.buf["vop"]
         vop[:, HEAD:] = jnp.ones((vop.shape[0], HEAD), BF)
 
+    def _row(self, dy):
+        return (self.me.y + dy) % 4
+
+    def _sums(self, m):
+        a = self.buf["acc"][m]
+        return a[:, :HEAD], jnp.transpose(a[:, HEAD:])[:8]
+
+    def _post(self, k, m, dst, slot, where, kind):
+        b, s = self.buf, self.sem
+        big, small = ("od", "dd") if kind == 1 else ("ro", "rd")
+        remote(b["ob"].at[m], b[big].at[dst], s["o_out"].at[0, k], s["o_in"].at[kind, 0, slot], where).start()
+        remote(b["db"].at[m], b[small].at[dst], s["o_out"].at[1, k], s["o_in"].at[kind, 1, slot], where).start()
+
+    def send_far_sums(self):
+        me, b = self.me, self.buf
+        for c, dy in ((0, 1), (1, 3)):
+            m = self._row(2) * 2 + c
+            o, d = self._sums(m)
+            b["ob"][m] = o.astype(BF)
+            b["db"][m] = d
+            self._post(c, m, c, c, (me.z, self._row(dy), me.c, me.t), 0)
+
     def send_sums(self):
         me, b, s = self.me, self.buf, self.sem
-        acc, ob, db, od, dd = (b[k] for k in ("acc", "ob", "db", "od", "dd"))
-
-        def halves(m):
-            a = acc[m]
-            return a[:, :HEAD].astype(BF), jnp.transpose(a[:, HEAD:])[:8]
-
-        def one(i, _):
-            m = (me.s8 + i) % SRC
-            ob[m], db[m] = halves(m)
-            where = me.at(me.z, m)
-            remote(ob.at[m], od.at[me.s8], s["o_out"].at[0], s["o_in"].at[0], where).start()
-            remote(db.at[m], dd.at[me.s8], s["o_out"].at[1], s["o_in"].at[1], where).start()
-            return 0
-
-        lax.fori_loop(1, SRC, one, 0)
-        od[me.s8], dd[me.s8] = halves(me.s8)
+        for c in (0, 1):
+            await_bytes(b["ro"].at[c], s["o_in"].at[0, 0, c])
+            await_bytes(b["rd"].at[c], s["o_in"].at[0, 1, c])
+        for side, dy in ((0, 1), (1, 3)):
+            for c in (0, 1):
+                m = self._row(dy) * 2 + c
+                o, d = self._sums(m)
+                if c == side:
+                    o = o + b["ro"][side].astype(F32)
+                    d = d + b["rd"][side]
+                b["ob"][m] = o.astype(BF)
+                b["db"][m] = d
+                into = 2 * side + me.c
+                self._post(2 + 2 * side + c, m, into, into, (me.z, self._row(dy), c, me.t), 1)
+        m = me.y * 2 + 1 - me.c
+        o, d = self._sums(m)
+        b["ob"][m] = o.astype(BF)
+        b["db"][m] = d
+        self._post(6, m, 4 + me.c, 4 + me.c, (me.z, me.y, 1 - me.c, me.t), 1)
+        o, d = self._sums(me.s8)
+        b["od"][4 + me.c] = o.astype(BF)
+        b["dd"][4 + me.c] = d
 
     def finish(self):
         b, s = self.buf, self.sem
         od, dd = b["od"], b["dd"]
         out_gain = self.ins[9]
-        await_bytes(od.at[pl.ds(0, SRC - 1)], s["o_in"].at[0])
-        await_bytes(dd.at[pl.ds(0, SRC - 1)], s["o_in"].at[1])
+        for k in range(4):
+            await_bytes(od.at[k], s["o_in"].at[1, 0, k])
+            await_bytes(dd.at[k], s["o_in"].at[1, 1, k])
+        await_bytes(od.at[0], s["o_in"].at[1, 0, 5 - self.me.c])
+        await_bytes(dd.at[0], s["o_in"].at[1, 1, 5 - self.me.c])
         for h in (0, 1):
-            o = sum(od[2 * y + h].astype(F32) for y in range(4))
-            d = sum(dd[2 * y + h] for y in range(4))
+            o = sum(od[2 * y + h].astype(F32) for y in range(3))
+            d = sum(dd[2 * y + h] for y in range(3))
             den = jnp.transpose(jnp.broadcast_to(d[0:1], (HEAD, d.shape[1])))
             m = o / den
             m = m * lax.rsqrt(jnp.mean(m * m, axis=-1, keepdims=True) + EPS) * out_gain[...]
@@ -335,8 +366,9 @@
                 for copy in self._copies(slot, up):
                     copy.wait_send()
 
-        await_bytes(b["od"].at[pl.ds(0, SRC - 1)], s["o_out"].at[0])
-        await_bytes(b["dd"].at[pl.ds(0, SRC - 1)], s["o_out"].at[1])
+        for k in range(7):
+            await_bytes(b["ob"].at[0], s["o_out"].at[0, k])
+            await_bytes(b["db"].at[0], s["o_out"].at[1, k])
 
 
 ATT_BUFS = {
@@ -351,10 +383,12 @@
     "vop": ((512, 256), "bf"),
     "ob": ((8, 256, 128), "bf"),
     "db": ((8, 8, 256), "f"),
-    "od": ((8, 256, 128), "bf"),
-    "dd": ((8, 8, 256), "f"),
+    "od": ((6, 256, 128), "bf"),
+    "dd": ((6, 8, 256), "f"),
+    "ro": ((2, 256, 128), "bf"),
+    "rd": ((2, 8, 256), "f"),
 }
-ATT_SEMS = {"kv_out": (2,), "kv_in": (8,), "rk_in": (8,), "q_out": None, "q_in": None, "hop_out": (8, 2), "o_out": (2,), "o_in": (2,)}
+ATT_SEMS = {"kv_out": (2,), "kv_in": (8,), "rk_in": (8,), "q_out": None, "q_in": None, "hop_out": (8, 2), "o_out": (2, 7), "o_in": (2, 2, 6)}
 
 
 def att_scratch():
@@ -564,21 +598,31 @@
         for k, step in ((0, 1), (1, 3)):
             remote(far.at[p, parts[k]], relay.at[p, parts[k]], rs_send.at[0, p, k], relay_sem.at[p, k], me.x(step)).start()
 
+    ways = ((to_r, from_l, fl_sem, 1), (to_l, from_r, fr_sem, 3))
+
+    def half_down(q, rank, h):
+        return dot(hid[q, parts[h]], wd[:, rank_cols(rank)])
+
+    def send_half(q, k, h, y):
+        buf, dst, sem, rank = ways[k]
+        buf[q, parts[h]] = y.astype(BF)
+        remote(buf.at[q, parts[h]], dst.at[q, parts[h]], rs_send.at[1 + k, q, h], sem.at[q, h], me.x(rank)).start()
+
+    def own_halves(q):
+        for k in (0, 1):
+            send_half(q, k, 1 - k, half_down(q, ways[k][3], 1 - k))
+
     def sides(q):
-        await_bytes(relay.at[q, parts[0]], relay_sem.at[q, 0])
-        await_bytes(relay.at[q, parts[1]], relay_sem.at[q, 1])
-        for k, (buf, dst, sem, rank) in enumerate(((to_r, from_l, fl_sem, 1), (to_l, from_r, fr_sem, 3))):
-            y = down(q, rank)
-            added = y[half * k : half * (k + 1)] + relay[q, parts[k]].astype(F32)
-            kept = y[half * (1 - k) : half * (2 - k)]
-            buf[q, parts[k]] = added.astype(BF)
-            buf[q, parts[1 - k]] = kept.astype(BF)
-            remote(buf.at[q], dst.at[q], rs_send.at[1 + k, q, 0], sem.at[q], me.x(rank)).start()
+        for k in (0, 1):
+            y = half_down(q, ways[k][3], k)
+            await_bytes(relay.at[q, parts[k]], relay_sem.at[q, k])
+            send_half(q, k, k, y + relay[q, parts[k]].astype(F32))
 
     def finish(q):
         y = down(q, 0)
-        await_bytes(from_l.at[q], fl_sem.at[q])
-        await_bytes(from_r.at[q], fr_sem.at[q])
+        for h in (0, 1):
+            await_bytes(from_l.at[q, parts[h]], fl_sem.at[q, h])
+            await_bytes(from_r.at[q, parts[h]], fr_sem.at[q, h])
         y = (y + from_l[q].astype(F32) + from_r[q].astype(F32)).astype(BF)
         ext = dot(pk_extra[...], y[:, 3 * 128 :])
         packed = dot(pk_main[...], y[:, : 3 * 128]) + jnp.concatenate([ext[256 * j : 256 * (j + 1)] for j in range(3)], axis=1)
@@ -637,17 +681,19 @@
             att.hop(0, True)
             att.hop(0, False)
 
+        last = jnp.where(me.z > DOWN - 1, PAIR_AT + DOWN - 1, jnp.where(me.z == 0, FIRST_AT, PAIR_AT + me.z - 1))
+
         @pl.when((k >= PAIR_AT) & (k < PAIR_AT + DOWN))
         def _():
             att.pairs(k - PAIR_AT + 1, False)
 
+        @pl.when((k >= 2) & (k < n_pairs + 2))
+        def _():
+            sides(k - 2)
+
         @pl.when((k >= 3) & (k < n_pairs + 3))
         def _():
             finish(k - 3)
-
-        @pl.when((k >= 2) & (k < n_pairs + 2))
-        def _():
-            sides(k - 2)
 
         @pl.when((k >= 1) & (k < n_pairs + 1))
         def _():
@@ -658,6 +704,7 @@
                 loads[2].wait()
 
             hidden_units(k - 1)
+            own_halves(k - 1)
 
         @pl.when(k == FIRST_AT)
         def _():
@@ -668,7 +715,11 @@
         def _():
             att.pairs(k - PAIR_AT + 1, True)
 
-        @pl.when(k == jnp.where(me.z > DOWN - 1, SUMS_AT, jnp.where(me.z == 0, FIRST_AT, PAIR_AT + me.z - 1)))
+        @pl.when(k == last)
+        def _():
+            att.send_far_sums()
+
+        @pl.when(k == last + 1)
         def _():
             att.send_sums()
 
@@ -699,7 +750,8 @@
     for q in range(4):
         for k in (0, 1):
             await_bytes(far.at[q, parts[k]], rs_send.at[0, q, k])
-            await_bytes(far.at[q], rs_send.at[1 + k, q, 0])
+            for h in (0, 1):
+                await_bytes(far.at[q, parts[h]], rs_send.at[1 + k, q, h])
     for b, k, n in ((0, 0, n_z), (0, 1, n_z), (1, 0, n_z // 2), (2, 1, n_z // 2)):
         await_bytes(arr.at[b, pl.ds(0, n)], xs_sem.at[b, k])
     for buf, sem in ((outb, out_sem), (retb, ret_send)):
@@ -716,6 +768,32 @@
     freqs = np.tile(freqs.astype(np.float32).astype(np.float64), 4)
     table = lambda at: jnp.asarray(np.stack([np.cos(at[:, None] * freqs), np.sin(at[:, None] * freqs)]), F32)
     return table(np.arange(NEAR)), table(np.arange(n_places) * NEAR)
+
+
+def settle(results):
+    count = len(results)
+
+    def body(*refs):
+        src, dst, held, sem = refs[:count], refs[count : 2 * count], refs[2 * count : 3 * count], refs[3 * count]
+        ins = [pltpu.make_async_copy(a, b, sem.at[0, k]) for k, (a, b) in enumerate(zip(src, held))]
+        outs = [pltpu.make_async_copy(a, b, sem.at[1, k]) for k, (a, b) in enumerate(zip(held, dst))]
+        for copy in ins:
+            copy.start()
+        for taken, copy in zip(ins, outs):
+            taken.wait()
+            copy.start()
+        for copy in outs:
+            copy.wait()
+
+    hbm = pl.BlockSpec(memory_space=pl.ANY)
+    return pl.pallas_call(
+        body,
+        out_shape=tuple(jax.ShapeDtypeStruct(a.shape, a.dtype) for a in results),
+        in_specs=[hbm] * count,
+        out_specs=(hbm,) * count,
+        scratch_shapes=[pltpu.VMEM(a.shape, a.dtype) for a in results] + [pltpu.SemaphoreType.DMA((2, count))],
+        name="settle",
+    )(*results)
 
 
 def on_device(
@@ -750,7 +828,7 @@
     small += (far, rope_key.T, row(moe_gain), routes.T, route_weights.T)
     big = (moe_tokens, queries, kv_latent, w_key_up, w_value_up, near, *fixed_selects())
     dma = pltpu.SemaphoreType.DMA
-    return pl.pallas_call(
+    results = pl.pallas_call(
         functools.partial(whole_kernel, n_z),
         out_shape=(
             jax.ShapeDtypeStruct((n_rows, 2 * HEAD), BF),
@@ -779,8 +857,8 @@
             dma((3, n_z)),
             dma((3, 4, 2)),
             dma((4, 2)),
-            dma((4,)),
-            dma((4,)),
+            dma((4, 2)),
+            dma((4, 2)),
             dma,
             dma,
             dma((3,)),
@@ -798,6 +876,7 @@
         w_up,
         w_down,
     )
+    return settle(results)
 
 
 def solution(mesh):

time: 106 us -> 105 us (level)
  local copies, waits for them, and re-layouts: 3.24 us -> 0 us
  Pallas kernels: 102 us -> 104 us
    unnamed x2 -> x0, local copies, waits for them, and re-layouts: 3.24 us -> none
    pallas_call x0 -> x1, Pallas kernels: none -> 1.76 us  [settle(): pl.pallas_call(body, out_shape=tuple((jax.ShapeDtypeStruct(a.shape, a.dty...]
where the time goes in v5:
time: 105 us
  Pallas kernels  104 us (99%)
    pallas_call x1, Pallas kernels, on_device(): pl.pallas_call(functools.partial(whole_kernel, n_z), out_shape=(jax.Shape...  102 us

profile of v5, /device:TPU:1, one launch (start us, length us, event | category | flops | bytes accessed | tf_op | source)
XLA Modules:
  0.0 104.5 jit_solution(4572475571658873526)
XLA Ops:
  0.6 102.1 %layer.1 = (bf16[256,256]{1,0:T(8,128)(2,1)}, bf16[64,2048]{1,0:T(8,128)(2,1)}) custom-call(f32[1,512]{1,0:T(1,128)} %bitcast.11, f32[1,192]{1,0:T(1,128)} %bitcast.14, f32[1,128]{1,0:T(1,128)} %bitcast.15, f32[1,64]{1,0:T(1,128)} %bitcast.16, f32[1,128]{1,0:T(1,128)} %bitcast.17, f32[2,64,128]{2,1,0:T(8,128)} %constant.13.clone.refs_5_, ...), custom_call_target="tpu_custom_call" | custom-call | tf_op jit(solution)/shard_map/layer/pallas_call | solution.py:831
  102.7 1.8 %settle.1 = (bf16[256,256]{1,0:T(8,128)(2,1)}, bf16[64,2048]{1,0:T(8,128)(2,1)}) custom-call(bf16[256,256]{1,0:T(8,128)(2,1)} %get-tuple-element.4.refs_0_, bf16[64,2048]{1,0:T(8,128)(2,1)} %get-tuple-element.5.refs_1_), custom_call_target="tpu_custom_call" | custom-call | tf_op jit(solution)/shard_map/settle/pallas_call | solution.py:789
